TPU v7x, 512 devices: a whole 4x8x8 slice. The times are simulated.
512 devices in a mesh: ep: 32 (over z, x), tp: 16 (over y, core).
Axes of the slice: x: 4, y: 8, z: 8, core: 2. Of those that a mesh axis runs over, the one named last changes fastest.
Arguments:
- x_in: bfloat16 [4096, 12288], P('tp', 'ep'), may hold values from -6 to 6
- z_in: bfloat16 [4096, 12288], P('tp', 'ep'), may hold values from -6 to 6
- dt_raw: float32 [64, 12288], P('tp', 'ep'), may hold values from -6 to 6
- decay_rate: float32 [64], P('tp'), may hold values from 0 to 1, as said below
- b_in: bfloat16 [256, 12288], P(None, 'ep'), may hold values from -6 to 6
- c_in: bfloat16 [256, 12288], P(None, 'ep'), may hold values from -6 to 6
- conv_x: float32 [4096, 4], P('tp'), may hold values from -3 to 3
- conv_b: float32 [256, 4], replicated, may hold values from -3 to 3
- conv_c: float32 [256, 4], replicated, may hold values from -3 to 3
- head_gain: float32 [4096], P('tp'), may hold values from 0.1 to 1.9
- moe_rows: bfloat16 [5120, 2048], P('ep'), may hold values from -6 to 6
- moe_gain: float32 [2048], replicated, may hold values from 0.1 to 1.9
- routes: int32 [5120, 2], P('ep'), may hold values from 0 to 31, all different within a row; in each aligned block of 160 rows (0 to 159, 160 to 319, ...) at most 20 rows name the same one
- route_logit: float32 [5120, 2], P('ep'), may hold values from -6 to 6
- w_gate: bfloat16 [32, 2048, 5120], P('ep', None, 'tp'), may hold values from -0.125 to 0.125
- w_up: bfloat16 [32, 2048, 5120], P('ep', None, 'tp'), may hold values from -0.125 to 0.125
- w_down: bfloat16 [32, 5120, 2048], P('ep', 'tp'), may hold values from -0.078125 to 0.078125
Outputs:
- mixed: bfloat16 [4096, 12288], P('tp', 'ep')
- moe_out: bfloat16 [2048, 5120], P('tp', 'ep')
Inputs may be any that keep to these rules, and one draw needn't show every extreme that they name: `routes`: each row names 2 different experts; among the rows of one index of ep no expert is named more than 20 times, a bound that some block reaches. `decay_rate`: positive rates.
All inputs are finite; a program needn't handle non-finite values.
Results may differ from a plain program's by a relative error of at most 0.018.
Values may be sent and summed in bfloat16 or wider, within the bound.
A program may use at most 64 MiB of HBM per device.

v0:
```python
import jax
import jax.numpy as jnp
from jax import lax
from jax.sharding import Mesh
from jax.sharding import PartitionSpec as P

HEADS = 64
HEAD_DIM = 64
GROUPS = 2
NSTATE = 128
BLOCK = 128
EXP_DEV = 1
EP = ("ep_0", "ep_1")


HIGHEST = lax.Precision.HIGHEST
ROW_EPS = 0.1
HEAD_EPS = 1.0


def from_behind(value, axis, steps):
    count = lax.axis_size(axis)
    initial, last = (max(0, -steps), min(count, count - steps))
    return lax.ppermute(value, axis, [(source, source + steps) for source in range(initial, last)])


def filled_with(shard, identity):
    return jax.tree.map(
        lambda a, e: jnp.broadcast_to(jnp.asarray(e, a.dtype), a.shape), shard, identity
    )


def entering(shard, axes, combine, identity):
    before = start = filled_with(shard, identity)
    total = shard
    for axis in reversed(axes):
        size, mine = (lax.axis_size(axis), lax.axis_index(axis))
        pieces = jax.tree.map(
            lambda part, kind: lax.all_gather(part.astype(kind), axis),
            total,
            (jnp.bfloat16, jnp.bfloat16),
        )
        inside, total = (start, start)
        for k in range(size):
            passed = k < mine
            total = combine(
                total, jax.tree.map(lambda part, own: part[k].astype(own.dtype), pieces, shard)
            )
            inside = jax.tree.map(lambda new, old: jnp.where(passed, new, old), total, inside)
        before = combine(inside, before)
    return before


def in_blocks(shard, dim, size):
    before, after = (shard.shape[:dim], shard.shape[dim + 1 :])
    return jnp.moveaxis(shard.reshape(*before, size, -1, *after), dim, 0)


def sent_and_summed(shard, axis, dim):
    tiles = in_blocks(shard, dim, lax.axis_size(axis))
    arrived = lax.all_to_all(tiles, axis, split_axis=0, concat_axis=0, tiled=True)
    return arrived.astype(jnp.float32).sum(axis=0)


def conv_with_rims(signal, rim_rows, weight):
    taps = weight.shape[1]
    length = signal.shape[1]
    joined = jnp.concatenate([rim_rows.astype(jnp.float32), signal.astype(jnp.float32)], axis=1)
    running = jnp.zeros(signal.shape, jnp.float32)
    for offset in range(taps):
        running = running + weight[:, offset : offset + 1] * joined[:, offset : offset + length]
    return jax.nn.silu(running)


def block_step(state_in, x_block, b_block, c_block, log_block, step_block):
    cum_log = jnp.cumsum(log_block, axis=1)
    seg_log = cum_log[:, :, None] - cum_log[:, None, :]
    causal = jnp.tril(jnp.ones((log_block.shape[1], log_block.shape[1]), bool))
    decay_mask = jnp.exp(jnp.where(causal[None], seg_log, -jnp.inf))
    scores = (
        jnp.einsum("hnt,hns->hts", c_block, b_block, precision=HIGHEST)
        * decay_mask
        * step_block[:, None, :]
    )
    inner_term = jnp.einsum("hts,hps->hpt", scores, x_block, precision=HIGHEST)
    carried = (
        jnp.einsum("hnt,hpn->hpt", c_block, state_in, precision=HIGHEST)
        * jnp.exp(cum_log)[:, None, :]
    )
    tail_weight = jnp.exp(cum_log[:, -1:] - cum_log) * step_block
    fresh_state = jnp.einsum(
        "hps,hns->hpn", x_block * tail_weight[:, None, :], b_block, precision=HIGHEST
    )
    new_state = jnp.exp(cum_log[:, -1])[:, None, None] * state_in + fresh_state
    return (new_state, inner_term + carried)


def combine_states(before_part, after_part):
    return (
        before_part[0] * after_part[0],
        after_part[0][..., None, None] * before_part[1] + after_part[1],
    )


def mixer_half(x_in, z_in, dt_raw, decay_rate, b_in, c_in, conv_x, conv_b, conv_c, head_gain):
    head_count = dt_raw.shape[0]
    length = dt_raw.shape[1]
    taps = conv_x.shape[1]
    value_rows = x_in.shape[0]
    per_group = HEADS // GROUPS
    group_index = lax.axis_index("tp") * head_count // per_group
    b_own = lax.dynamic_slice_in_dim(b_in, group_index * NSTATE, NSTATE, 0)
    c_own = lax.dynamic_slice_in_dim(c_in, group_index * NSTATE, NSTATE, 0)
    taps_b = lax.dynamic_slice_in_dim(conv_b, group_index * NSTATE, NSTATE, 0)
    taps_c = lax.dynamic_slice_in_dim(conv_c, group_index * NSTATE, NSTATE, 0)
    edge = length - taps + 1
    own_rims = jnp.concatenate([x_in[:, edge:], b_own[:, edge:], c_own[:, edge:]], axis=0)
    rims = from_behind(own_rims, EP, 1)
    x_conv = conv_with_rims(x_in, rims[:value_rows], conv_x).reshape(head_count, HEAD_DIM, length)
    b_conv = conv_with_rims(b_own, rims[value_rows : value_rows + NSTATE], taps_b)
    c_conv = conv_with_rims(c_own, rims[value_rows + NSTATE :], taps_c)
    step_dt = jax.nn.softplus(dt_raw)
    log_decay = -step_dt * decay_rate[:, None]
    block_count = length // BLOCK

    def blocks(tensor):
        return jnp.moveaxis(tensor.reshape(tensor.shape[:-1] + (block_count, BLOCK)), -2, 0)

    def spread_heads(tensor):
        return jnp.broadcast_to(tensor[None], (head_count,) + tensor.shape)

    def advance(state_in, inputs):
        x_block, b_block, c_block, log_block, step_block = inputs
        return block_step(
            state_in, x_block, spread_heads(b_block), spread_heads(c_block), log_block, step_block
        )

    init_state = jnp.zeros((head_count, HEAD_DIM, NSTATE), jnp.float32)
    local_state, block_out = lax.scan(
        advance,
        init_state,
        (blocks(x_conv), blocks(b_conv), blocks(c_conv), blocks(log_decay), blocks(step_dt)),
    )
    y_local = jnp.moveaxis(block_out, 0, -2).reshape(head_count, HEAD_DIM, length)
    total_decay = jnp.exp(jnp.sum(log_decay, axis=1))
    _, incoming = entering(
        (total_decay, local_state),
        EP,
        combine_states,
        (jnp.ones_like(total_decay), jnp.zeros_like(local_state)),
    )
    reach_decay = jnp.exp(jnp.cumsum(log_decay, axis=1))
    carried = (
        jnp.einsum("nt,hpn->hpt", c_conv, incoming, precision=HIGHEST) * reach_decay[:, None, :]
    )
    y_mixed = y_local + carried
    gated_out = y_mixed * jax.nn.silu(
        z_in.astype(jnp.float32).reshape(head_count, HEAD_DIM, length)
    )
    head_scale = lax.rsqrt(jnp.mean(gated_out * gated_out, axis=1, keepdims=True) + HEAD_EPS)
    normed_out = gated_out * head_scale * head_gain.reshape(head_count, HEAD_DIM, 1)
    return normed_out.reshape(head_count * HEAD_DIM, length).astype(jnp.bfloat16)


def experts_half(moe_rows, moe_gain, routes, route_logit, w_gate, w_up, w_down):
    tokens = moe_rows.shape[0]
    top_count = routes.shape[1]
    features = moe_gain.shape[0]
    experts = EXP_DEV * lax.axis_size(EP)
    capacity = 2 * tokens * top_count // experts
    col_width = features // lax.axis_size("tp")
    rows_float = moe_rows.astype(jnp.float32)
    row_scale = lax.rsqrt(jnp.mean(rows_float * rows_float, axis=1, keepdims=True) + ROW_EPS)
    normed_float = rows_float * row_scale * moe_gain
    flat_routes = routes.reshape(-1)
    hit_table = (flat_routes[:, None] == jnp.arange(experts, dtype=jnp.int32)[None, :]).astype(
        jnp.int32
    )
    slot_rank = jnp.sum((jnp.cumsum(hit_table, axis=0) - hit_table) * hit_table, axis=1)
    slot_index = flat_routes * capacity + slot_rank
    owner_row = jnp.arange(tokens * top_count, dtype=jnp.int32) // top_count
    column = lax.axis_index("tp") * col_width
    normed = lax.dynamic_slice_in_dim(normed_float.astype(jnp.bfloat16), column, col_width, 1)
    outbox = (
        jnp.zeros((experts * capacity, col_width), jnp.bfloat16)
        .at[slot_index]
        .set(normed[owner_row])
    )
    arrived = lax.all_to_all(
        outbox.reshape(experts, capacity, col_width), EP, split_axis=0, concat_axis=0, tiled=True
    ).reshape(-1, col_width)
    part_rows = lax.all_gather(arrived, "tp", axis=1, tiled=True)
    gate_rows = w_gate[0]
    up_rows = w_up[0]
    gate_act = jnp.dot(part_rows, gate_rows, preferred_element_type=jnp.float32)
    up_act = jnp.dot(part_rows, up_rows, preferred_element_type=jnp.float32)
    hidden = (jax.nn.silu(gate_act) * up_act).astype(jnp.bfloat16)
    columns = w_down[0]
    summed = sent_and_summed(
        lax.dot_general(
            columns, hidden, (((0,), (1,)), ((), ())), preferred_element_type=jnp.float32
        ).astype(jnp.bfloat16),
        "tp",
        0,
    )
    expert_out = summed.astype(jnp.bfloat16).reshape(col_width, experts, capacity)
    returned = lax.all_to_all(expert_out, EP, split_axis=1, concat_axis=1, tiled=True)
    picked = returned.reshape(col_width, experts * capacity)[:, slot_index].astype(jnp.float32)
    picked = picked.reshape(col_width, tokens, top_count)
    weight = jax.nn.sigmoid(route_logit - route_logit[:, ::-1])
    combined = jnp.sum(picked * weight[None], axis=2)
    return combined.astype(jnp.bfloat16)


def on_device(
    x_in,
    z_in,
    dt_raw,
    decay_rate,
    b_in,
    c_in,
    conv_x,
    conv_b,
    conv_c,
    head_gain,
    moe_rows,
    moe_gain,
    routes,
    route_logit,
    w_gate,
    w_up,
    w_down,
):
    mixed = mixer_half(
        x_in, z_in, dt_raw, decay_rate, b_in, c_in, conv_x, conv_b, conv_c, head_gain
    )
    moe_out = experts_half(moe_rows, moe_gain, routes, route_logit, w_gate, w_up, w_down)
    return (mixed, moe_out)


def solution(mesh):
    finer = Mesh(mesh.devices.reshape(8, 4, mesh.shape["tp"]), ("ep_0", "ep_1", "tp"))
    in_specs = (
        P("tp", EP),
        P("tp", EP),
        P("tp", EP),
        P("tp"),
        P(None, EP),
        P(None, EP),
        P("tp", None),
        P(),
        P(),
        P("tp"),
        P(EP, None),
        P(),
        P(EP, None),
        P(EP, None),
        P(EP, None, "tp"),
        P(EP, None, "tp"),
        P(EP, "tp", None),
    )
    out_specs = (P("tp", EP), P("tp", EP))
    return jax.shard_map(
        on_device, mesh=finer, in_specs=in_specs, out_specs=out_specs, check_vma=False
    )
```

profile of v0, /device:TPU:6, one launch (start us, length us, event | category | flops | bytes accessed | tf_op | source)
XLA Modules:
  0.0 192.7 jit_solution(6418290742828513007)
XLA Ops:
  7.2 1.3 convert_element_type.375
  8.6 0.2 multiply_reduce_fusion
  9.2 0.9 reduce-window.16
  10.0 0.2 slice_reduce_fusion.1
  10.8 0.8 dynamic-slice.1
  11.7 2.1 %scatter_custom_fusion = bf16[640,128]{1,0:T(8,128)(2,1)S(1)} fusion(s32[320]{0:T(512)S(1)} %get-tuple-element.144, bf16[160,128]{1,0:T(8,128)(2,1)S(1)} %fusion.96, s32[1024]{0:T(1024)S(1)} %pad_clamp_fusion.1, bf16[]{:T(256)} %constant.124.clone.1), kind=kCustom, calls=%fused_computation.142 | custom fusion | bytes 163842 | tf_op jit(solution)/shard_map/scatter | solution.py:187
  13.9 23.2 %all_to_all.15 = bf16[32,20,128]{2,1,0:T(8,128)(2,1)S(1)} all-to-all(bf16[32,20,128]{2,1,0:T(8,128)(2,1)S(1)} %reshape.360), channel_id=1, replica_groups=mesh['ep_0'=8,'ep_1'=4,'tp'=16] {'ep_0','ep_1'}, dimensions={0} | all-to-all | bytes 327680 | tf_op jit(solution)/shard_map/all_to_all | solution.py:189
  37.0 0.7 reshape.361
  37.8 0.9 constant_dynamic-slice_fusion.5
  39.2 1.3 dynamic-slice
  41.4 0.2 dynamic-update-slice
  41.6 4.3 %collective-permute-start = (bf16[512,3]{0,1:T(4,128)(2,1)S(1)}, bf16[512,3]{0,1:T(4,128)(2,1)S(1)}, u32[]{:S(2)}, u32[]{:S(2)}) collective-permute-start(bf16[512,3]{0,1:T(4,128)(2,1)S(1)} %pad_maximum_fusion.3), channel_id=1, source_target_pairs={{0,16},{16,32},{32,48},{48,64},{64,80},{80,96},{96,112},{112,128},... | collective-permute-start | bytes 9224 | tf_op jit(solution)/shard_map/ppermute | solution.py:24
  45.9 7.5 %all-reduce.1 = bf16[16]{0:T(256)(128)(2,1)S(1)} all-reduce(bf16[16]{0:T(256)(128)(2,1)S(1)} %dynamic-update-slice), channel_id=2, replica_groups=mesh['ep_0'=8,'ep_1'=4,'tp'=16] {'ep_1'}, use_global_device_ids=true, to_apply=%add.1 | all-reduce | flops 16 | bytes 64
  53.4 13.9 %all-gather.2 = bf16[8,1,4]{2,1,0:T(2,128)(2,1)S(1)} all-gather(bf16[1,1,4]{2,1,0:T(2,128)(2,1)S(1)} %bitcast.294), channel_id=1, replica_groups=mesh['ep_0'=8,'ep_1'=4,'tp'=16] {'ep_0'}, dimensions={0}, use_global_device_ids=true | all-gather | bytes 72 | tf_op jit(solution)/shard_map/all_gather | solution.py:39
  67.3 1.2 reduce-window.14
  69.7 0.6 divide_multiply_fusion
  70.8 8.7 %all-gather.5.cloned.1.call-done = bf16[640,2048]{1,0:T(8,128)(2,1)} async-done(((bf16[640,128]{1,0:T(8,128)(2,1)}), bf16[640,2048]{1,0:T(8,128)(2,1)}) %all-gather.5.cloned.1.call-update) | async-done | bytes 2621456 | tf_op jit(solution)/shard_map/all_gather | solution.py:192
  79.5 4.3 %fusion.19 = f32[640,320]{0,1:T(8,128)} fusion(bf16[640,2048]{1,0:T(8,128)(2,1)} %all-gather.5.cloned.1.call-done, bf16[1,2048,320]{1,2,0:T(8,128)(2,1)} %param.33), kind=kOutput, calls=%fused_computation.35 | convolution fusion | flops 838860800 | bytes 4751360 | tf_op jit(solution)/shard_map/dot_general | solution.py:195
  83.7 7.1 %fusion.15 = bf16[80,16,8,128]{3,2,1,0:T(8,128)(2,1)} fusion(bf16[1,320,2048]{2,1,0:T(8,128)(2,1)S(1)} %copy-done, bf16[640,2048]{1,0:T(8,128)(2,1)} %all-gather.5.cloned.1.call-done, bf16[1,2048,320]{1,2,0:T(8,128)(2,1)} %param.34, f32[640,320]{0,1:T(8,128)} %fusion.19), kind=kOutput, calls=%fused_computation.31 | convolution fusion | flops 1680261120 | bytes 8683520 | tf_op jit(solution)/shard_map/dot_general | solution.py:200
  90.9 3.9 %copy.73 = bf16[80,16,8,128]{3,2,0,1:T(8,128)(2,1)} copy(bf16[80,16,8,128]{3,2,1,0:T(8,128)(2,1)} %fusion.15) | data formatting | bytes 5242880 | tf_op jit(solution)/shard_map/reshape | solution.py:56
  94.8 5.2 %all-to-all-start.1 = ((bf16[16,128,640]{1,2,0:T(8,128)(2,1)}), bf16[16,128,640]{1,2,0:T(8,128)(2,1)}, u32[]{:S(2)}, u32[]{:S(2)}) async-start(bf16[16,128,640]{1,2,0:T(8,128)(2,1)} %bitcast.276), calls=%async_computation.1 | async-start | bytes 5242880 | tf_op jit(solution)/shard_map/all_to_all | solution.py:61
  100.0 9.7 %while.13 = (s32[]{:T(128)}, f32[4,64,128]{2,1,0:T(8,128)S(1)}, f32[3,4,64,128]{3,2,1,0:T(8,128)S(1)}, f32[3,4,128]{2,1,0:T(4,128)S(1)}, f32[3,4,64,128]{3,0,2,1...) while((s32[]{:T(128)}, f32[4,64,128]{2,1,0:T(8,128)S(1)}, ...), condition=%wide.region_2.3_spmd.clone, body=%wide.region_0.2_spmd.clone.sunk | while | flops 252232192 | bytes 2681072 | solution.py:139
  100.0 0.3 reduce_window_sum.51
  100.8 0.6 fusion.178
  101.6 0.6 fusion.179
  102.2 0.3 fusion.180
  102.6 0.6 convolution_add_fusion.2
  103.2 0.3 reduce_window_sum.51
  104.0 0.6 fusion.178
  104.8 0.6 fusion.179
  105.4 0.3 fusion.180
  105.8 0.6 convolution_add_fusion.2
  106.5 0.3 reduce_window_sum.51
  107.3 0.6 fusion.178
  108.0 0.6 fusion.179
  108.7 0.3 fusion.180
  109.0 0.6 convolution_add_fusion.2
  109.7 12.4 %all-gather.1 = bf16[16,64,128]{2,1,0:T(8,128)(2,1)S(1)} all-gather(bf16[4,64,128]{2,1,0:T(8,128)(2,1)S(1)} %convert_element_type.342), channel_id=3, replica_groups=mesh['ep_0'=8,'ep_1'=4,'tp'=16] {'ep_1'}, dimensions={0}, use_global_device_ids=true | all-gather | bytes 327680 | tf_op jit(solution)/shard_map/all_gather | solution.py:39
  122.2 27.4 %all_gather.25 = bf16[8,4,64,128]{3,2,1,0:T(8,128)(2,1)S(1)} all-gather(bf16[1,4,64,128]{3,2,1,0:T(8,128)(2,1)S(1)} %fusion.74), channel_id=1, replica_groups=mesh['ep_0'=8,'ep_1'=4,'tp'=16] {'ep_0'}, dimensions={0}, use_global_device_ids=true | all-gather | bytes 589824 | tf_op jit(solution)/shard_map/all_gather | solution.py:39
  149.6 0.8 multiply_reduce_fusion.1
  150.4 10.1 %all-to-all-done.1 = bf16[16,128,640]{1,2,0:T(8,128)(2,1)} async-done(((bf16[16,128,640]{1,2,0:T(8,128)(2,1)}), bf16[16,128,640]{1,2,0:T(8,128)(2,1)}, u32[]{:S(2)}, u32[]{:S(2)}) %all-to-all-start.1) | async-done | bytes 2621472 | tf_op jit(solution)/shard_map/all_to_all | solution.py:61
  160.5 2.1 %reduce_sum.64 = bf16[128,640]{0,1:T(8,128)(2,1)S(1)} reduce(bf16[16,128,640]{1,2,0:T(8,128)(2,1)} %all-to-all-done.1, bf16[]{:T(256)} %constant.124.clone.1), dimensions={0}, to_apply=%region_12.13 | reduce | flops 1228800 | bytes 2785282 | tf_op jit(solution)/shard_map/reduce_sum | solution.py:62
  162.7 0.7 reshape.363
  163.4 10.4 %all-to-all-start.2 = ((bf16[128,32,20]{0,2,1:T(8,128)(2,1)}), bf16[128,32,20]{0,2,1:T(8,128)(2,1)S(1)}, u32[]{:S(2)}, u32[]{:S(2)}) async-start(bf16[128,32,20]{0,2,1:T(8,128)(2,1)} %reshape.363), calls=%async_computation.2 | async-start | bytes 393216 | tf_op jit(solution)/shard_map/all_to_all | solution.py:207
  173.8 0.8 multiply_convert_fusion
  174.5 8.9 %all-to-all-done.2 = bf16[128,32,20]{0,2,1:T(8,128)(2,1)S(1)} async-done(((bf16[128,32,20]{0,2,1:T(8,128)(2,1)}), bf16[128,32,20]{0,2,1:T(8,128)(2,1)S(1)}, u32[]{:S(2)}, u32[]{:S(2)}) %all-to-all-start.2) | async-done | bytes 163872 | tf_op jit(solution)/shard_map/all_to_all | solution.py:207
  183.5 1.4 gather_fusion
  185.0 0.9 multiply_reduce_fusion.2
  (115 shorter events, 5.1 us)
Async XLA Ops:
  7.2 76.6 %copy-start = (bf16[1,320,2048]{2,1,0:T(8,128)(2,1)S(1)}, bf16[1,320,2048]{2,1,0:T(8,128)(2,1)}, u32[]{:S(2)}) copy-start(bf16[1,320,2048]{2,1,0:T(8,128)(2,1)} %param.35) | copy-start | bytes 3932164
  7.2 1.4 copy-start.1
  7.2 72.3 %all-gather.5.cloned.1.call-start = ((), (), s32[]{:S(2)}) async-start(), calls=%async_computation.3 | async-start | bytes 2785280 | tf_op jit(solution)/shard_map/all_gather | solution.py:192
  7.2 1.6 copy-start.5
  8.8 29.0 %copy-start.3 = (bf16[256,384]{1,0:T(8,128)(2,1)S(1)}, bf16[256,384]{1,0:T(8,128)(2,1)}, u32[]{:S(2)}) copy-start(bf16[256,384]{1,0:T(8,128)(2,1)} %param.24) | copy-start | bytes 589828
  10.4 28.6 %copy-start.2 = (bf16[256,384]{1,0:T(8,128)(2,1)S(1)}, bf16[256,384]{1,0:T(8,128)(2,1)}, u32[]{:S(2)}) copy-start(bf16[256,384]{1,0:T(8,128)(2,1)} %param.19) | copy-start | bytes 589828
  10.7 30.4 %copy-start.6 = (f32[4,384]{1,0:T(4,128)S(1)}, f32[4,384]{1,0:T(4,128)}, u32[]{:S(2)}) copy-start(f32[4,384]{1,0:T(4,128)} %param.21) | copy-start | bytes 18436
  10.7 30.4 %copy-start.11 = (f32[4]{0:T(128)S(1)}, f32[4]{0:T(128)}, u32[]{:S(2)}) copy-start(f32[4]{0:T(128)} %param.22) | copy-start | bytes 52
  11.6 57.3 %copy-start.4 = (f32[160,2]{0,1:T(2,128)S(1)}, f32[160,2]{0,1:T(2,128)}, u32[]{:S(2)}) copy-start(f32[160,2]{0,1:T(2,128)} %param.32) | copy-start | bytes 3844
  11.6 57.3 %copy-start.8 = (f32[256,4]{0,1:T(4,128)S(1)}, f32[256,4]{0,1:T(4,128)}, u32[]{:S(2)}) copy-start(f32[256,4]{0,1:T(4,128)} %param.27) | copy-start | bytes 12292
  11.6 57.3 %copy-start.9 = (f32[256,4]{0,1:T(4,128)S(1)}, f32[256,4]{0,1:T(4,128)}, u32[]{:S(2)}) copy-start(f32[256,4]{0,1:T(4,128)} %param.26) | copy-start | bytes 12292
  11.7 57.5 %copy-start.7 = (f32[256,4]{0,1:T(4,128)S(1)}, f32[256,4]{0,1:T(4,128)}, u32[]{:S(2)}) copy-start(f32[256,4]{0,1:T(4,128)} %param.25) | copy-start | bytes 12292
  37.8 31.6 %copy-start.10 = (f32[256]{0:T(256)S(1)}, f32[256]{0:T(256)}, u32[]{:S(2)}) copy-start(f32[256]{0:T(256)} %param.28) | copy-start | bytes 3076
  41.6 28.0 %collective-permute-start = (bf16[512,3]{0,1:T(4,128)(2,1)S(1)}, bf16[512,3]{0,1:T(4,128)(2,1)S(1)}, u32[]{:S(2)}, u32[]{:S(2)}) collective-permute-start(bf16[512,3]{0,1:T(4,128)(2,1)S(1)} %pad_maximum_fusion.3), channel_id=1, source_target_pairs={{0,16},{16,32},{32,48},{48,64},{64,80},{80,96},{96,112},{112,128},... | collective-permute-start | bytes 9224 | tf_op jit(solution)/shard_map/ppermute | solution.py:24
  94.8 65.7 %all-to-all-start.1 = ((bf16[16,128,640]{1,2,0:T(8,128)(2,1)}), bf16[16,128,640]{1,2,0:T(8,128)(2,1)}, u32[]{:S(2)}, u32[]{:S(2)}) async-start(bf16[16,128,640]{1,2,0:T(8,128)(2,1)} %bitcast.276), calls=%async_computation.1 | async-start | bytes 5242880 | tf_op jit(solution)/shard_map/all_to_all | solution.py:61
  109.7 39.9 %copy-start.12 = (bf16[256,384]{1,0:T(8,128)(2,1)S(1)}, bf16[256,384]{1,0:T(8,128)(2,1)}, u32[]{:S(2)}) copy-start(bf16[256,384]{1,0:T(8,128)(2,1)} %param.20) | copy-start | bytes 589828
  163.4 20.1 %all-to-all-start.2 = ((bf16[128,32,20]{0,2,1:T(8,128)(2,1)}), bf16[128,32,20]{0,2,1:T(8,128)(2,1)S(1)}, u32[]{:S(2)}, u32[]{:S(2)}) async-start(bf16[128,32,20]{0,2,1:T(8,128)(2,1)} %reshape.363), calls=%async_computation.2 | async-start | bytes 393216 | tf_op jit(solution)/shard_map/all_to_all | solution.py:207
Sparse Core Ops, SparseCore 0:
  37.9 41.5 all-gather.4
where the time goes:
time: 195 us; the launch traced here: 193 us
  blocking collectives  84.4 us (43%)
  waiting for transfers between devices  27.7 us (14%)
  starting transfers between devices  19.8 us (10%)
  matrix products  18.8 us (10%)
  local copies, waits for them, and re-layouts  15.7 us (8%)
  between operations  15.3 us (8%)
  other arithmetic  10.7 us (5%)
    all_gather x3, blocking collectives, entering(): lax.all_gather(part.astype(kind), axis)  53.7 us
    all_to_all x1, blocking collectives, experts_half(): lax.all_to_all(outbox.reshape(experts, capacity, col_width), EP, split_ax...  23.2 us
    all_to_all x1, starting transfers between devices, experts_half(): lax.all_to_all(expert_out, EP, split_axis=1, concat_axis=1, tiled=True)  10.4 us
    all_to_all x1, waiting for transfers between devices, sent_and_summed(): lax.all_to_all(tiles, axis, split_axis=0, concat_axis=0, tiled=True)  10.1 us
    all_to_all x1, waiting for transfers between devices, experts_half(): lax.all_to_all(expert_out, EP, split_axis=1, concat_axis=1, tiled=True)  8.95 us
    all_gather x1, waiting for transfers between devices, experts_half(): part_rows = lax.all_gather(arrived, 'tp', axis=1, tiled=True)  8.67 us
    unnamed x1, blocking collectives  7.49 us
    dot_general x1, matrix products, experts_half(): lax.dot_general(columns, hidden, (((0,), (1,)), ((), ())), preferred_elem...  7.12 us
  transfers between devices with their start and end apart: 4, of which 3 were waited for; matrix products, arithmetic and copies ran while one was open for 9% of the time, Pallas kernels for 0%

commit v1 on v0

v1 whole, which is shorter than its diff:
```python
import functools

import jax
import jax.numpy as jnp
from jax import lax
from jax.experimental import pallas as pl
from jax.experimental.pallas import tpu as pltpu
from jax.sharding import PartitionSpec as P

F32 = jnp.float32
BF16 = jnp.bfloat16
MESH = pl.DeviceIdType.MESH
HIGHEST = lax.Precision.HIGHEST
GROUPS = 2
NSTATE = 128
LANES = 128
QUAD = 4
ROW_EPS = 0.1
HEAD_EPS = 1.0


def mm(a, b, dims=(((1,), (0,)), ((), ()))):
    return lax.dot_general(a, b, dims, preferred_element_type=F32)


def kernel_body(
    cfg,
    x_hbm, z_hbm, dt_ref, rate_ref, b_hbm, c_hbm, tapx_ref, tapb_ref, tapc_ref, hgain_ref,
    rows_hbm, mgain_ref, routes_ref, logit_ref, wg_hbm, wu_hbm, wd_hbm,
    mixed_ref, moe_ref,
    x_v, z_v, b_v, c_v, rows_v, wg_v, wu_v, wd_v, halo, pick, outbox, xall,
    gate_acc, up_acc, hid, part, sib, tosend, arrived, rout, rin,
    xs_v, bc_v, cc_v, cum_v, colv, yloc, sout, sin, hout, hin,
    load_sem, halo_send, halo_recv, disp_send, disp_recv, st_send, st_recv, hb_send, hb_recv,
    ag_send, ag_recv, d2_send, d2_recv, ps_send, ps_recv, rs_send, rs_recv, rt_send, rt_recv,
):
    EP, TP, CAP, L, HH = cfg["EP"], cfg["TP"], cfg["CAP"], cfg["L"], cfg["HH"]
    NY = TP // 2
    UC = CAP // QUAD
    ROWS = EP * CAP
    HALF = ROWS // QUAD // 2
    tokens = rows_v.shape[0]
    VR = x_v.shape[0]
    HD = VR // HH
    NB = L // LANES
    U = VR // EP
    UR = sout.shape[1]
    ep, tp = lax.axis_index("ep"), lax.axis_index("tp")
    y, core = lax.div(tp, 2), lax.rem(tp, 2)
    other = 1 - core
    group = lax.div(tp, TP // GROUPS)

    def to_ep(d):
        return {"ep": lax.rem(ep + d, EP), "tp": tp}

    def to_y(s):
        return {"ep": ep, "tp": lax.rem(y + s + NY, NY) * 2 + core}

    sibling = {"ep": ep, "tp": y * 2 + other}

    def rcopy(src, dst, ssem, rsem, dev):
        return pltpu.make_async_remote_copy(
            src_ref=src, dst_ref=dst, send_sem=ssem, recv_sem=rsem, device_id=dev, device_id_type=MESH
        )

    def flat(block):
        return block.reshape(block.shape[0] * QUAD, LANES)

    def put(ref, value):
        ref[...] = value.reshape(value.shape[0] // QUAD, QUAD, LANES)

    def wait_bytes(ref, sem):
        pltpu.make_async_copy(ref, ref, sem).wait()

    gsel = pl.ds(pl.multiple_of(group * NSTATE, NSTATE), NSTATE)
    loads = [
        pltpu.make_async_copy(src, dst, load_sem.at[i])
        for i, (src, dst) in enumerate(
            (
                (rows_hbm, rows_v), (x_hbm, x_v), (b_hbm.at[gsel, :], b_v), (c_hbm.at[gsel, :], c_v),
                (wg_hbm.at[0], wg_v), (wu_hbm.at[0], wu_v), (wd_hbm.at[0], wd_v), (z_hbm, z_v),
            )
        )
    ]
    for load in loads:
        load.start()

    barrier = pltpu.get_barrier_semaphore()

    @pl.loop(1, EP)
    def _(d):
        pl.semaphore_signal(barrier, inc=1, device_id=to_ep(d), device_id_type=MESH)

    for dev in (to_y(1), to_y(-1), sibling):
        pl.semaphore_signal(barrier, inc=1, device_id=dev, device_id_type=MESH)

    routes = routes_ref[...]
    lane_e = lax.broadcasted_iota(jnp.int32, (tokens, EP), 1)
    hits = [(routes[:, k : k + 1] == lane_e).astype(F32) for k in range(2)]
    below = (
        lax.broadcasted_iota(jnp.int32, (tokens, tokens), 0)
        > lax.broadcasted_iota(jnp.int32, (tokens, tokens), 1)
    ).astype(BF16)
    ahead = mm(below, (hits[0] + hits[1]).astype(BF16))
    lane_s = lax.broadcasted_iota(jnp.int32, (tokens, ROWS), 1)
    onehot = None
    for k in range(2):
        rank = jnp.sum(ahead * hits[k], axis=1, keepdims=True).astype(jnp.int32)
        slot = routes[:, k : k + 1] * CAP + rank
        hot = (lane_s == slot).astype(F32)
        pick[k] = hot.astype(BF16)
        onehot = hot if onehot is None else onehot + hot

    loads[0].wait()
    rows_f = rows_v[...].astype(F32)
    row_scale = lax.rsqrt(jnp.mean(rows_f * rows_f, axis=1, keepdims=True) + ROW_EPS)
    own_cols = rows_v[:, pl.ds(pl.multiple_of(tp * LANES, LANES), LANES)].astype(F32)
    normed = (own_cols * row_scale * mgain_ref[pl.ds(tp, 1), :]).astype(BF16)
    packed = mm(onehot.astype(BF16), normed, (((0,), (0,)), ((), ()))).astype(BF16)
    put(outbox, packed)

    for i in (1, 2, 3):
        loads[i].wait()
    pl.semaphore_wait(barrier, EP - 1 + 3)

    @pl.loop(1, EP)
    def _(d):
        tgt = lax.rem(ep + d, EP)
        rcopy(
            outbox.at[pl.ds(tgt * UC, UC)], xall.at[tp, pl.ds(ep * UC, UC)], disp_send, disp_recv, to_ep(d)
        ).start()

    last = pl.ds(L - LANES, LANES)
    halos = [
        rcopy(x_v.at[:, last], halo.at[pl.ds(0, VR)], halo_send.at[0], halo_recv.at[0], to_ep(1)),
        rcopy(b_v.at[:, last], halo.at[pl.ds(VR, NSTATE)], halo_send.at[1], halo_recv.at[1], to_ep(1)),
        rcopy(
            c_v.at[:, last], halo.at[pl.ds(VR + NSTATE, NSTATE)], halo_send.at[2], halo_recv.at[2], to_ep(1)
        ),
    ]
    for h in halos:
        h.start()
    xall[tp, pl.ds(ep * UC, UC)] = outbox[pl.ds(ep * UC, UC)]

    dt = dt_ref[...]
    step = jnp.maximum(dt, 0.0) + jnp.log1p(jnp.exp(-jnp.abs(dt)))
    head_row = lax.broadcasted_iota(jnp.int32, (HH, L), 0)
    rate = jnp.zeros((HH, L), F32)
    for h in range(HH):
        rate = jnp.where(head_row == h, rate_ref[h], rate)
    logd = -step * rate
    upper = (
        lax.broadcasted_iota(jnp.int32, (LANES, LANES), 0)
        <= lax.broadcasted_iota(jnp.int32, (LANES, LANES), 1)
    ).astype(F32)
    pieces, carry = [], jnp.zeros((HH, 1), F32)
    for k in range(NB):
        piece = (
            jnp.dot(
                logd[:, k * LANES : (k + 1) * LANES], upper, precision=HIGHEST, preferred_element_type=F32
            )
            + carry
        )
        carry = piece[:, LANES - 1 : LANES]
        pieces.append(piece)
    cum = jnp.concatenate(pieces, axis=1)
    total = carry
    cum_v[pl.ds(0, HH), :] = cum
    tall = jnp.concatenate([cum, jnp.zeros((8 - HH, L), F32)], axis=0)
    colv[...] = jnp.transpose(tall)

    for h in halos:
        h.wait_recv()
    started = (ep > 0).astype(F32)

    def conv(cur, rim, taps):
        joined = jnp.concatenate([rim.astype(F32) * started, cur.astype(F32)], axis=1)
        out = taps[:, 3:4] * joined[:, LANES:]
        for k in range(3):
            out = out + taps[:, k : k + 1] * pltpu.roll(joined, 3 - k, 1)[:, LANES:]
        return out * jax.nn.sigmoid(out)

    b_conv = conv(b_v[...], halo[pl.ds(VR, NSTATE), :], tapb_ref[gsel, :]).astype(BF16)
    bc_v[...] = b_conv
    tail = jnp.exp(total - cum)
    for h in range(HH):
        rows_h = pl.ds(h * HD, HD)
        xc = conv(x_v[rows_h, :], halo[rows_h, :], tapx_ref[rows_h, :])
        xs = xc * step[h : h + 1, :]
        xs_v[rows_h, :] = xs.astype(BF16)
        yloc[rows_h, :] = xs * tail[h : h + 1, :]
    state = mm(yloc[...].astype(BF16), b_conv, (((1,), (1,)), ((), ())))

    hi = total.astype(BF16).astype(F32)
    mid = (total - hi).astype(BF16).astype(F32)
    low = total - hi - mid
    r8 = lax.broadcasted_iota(jnp.int32, (8, LANES), 0)
    decays = []
    for u in range(EP):
        h = u * U // HD
        decays.append(
            jnp.where(
                r8 == 0,
                hi[h : h + 1],
                jnp.where(r8 == 1, mid[h : h + 1], jnp.where(r8 == 2, low[h : h + 1], 0.0)),
            )
        )
    for u in range(EP):
        extra = [state[u * U : (u + 1) * U], decays[u]]
        if UR > U + 8:
            extra.append(jnp.zeros((UR - U - 8, LANES), F32))
        sout[u] = jnp.concatenate(extra, axis=0).astype(BF16)

    @pl.loop(1, EP)
    def _(d):
        tgt = lax.rem(ep + d, EP)
        rcopy(sout.at[tgt], sin.at[ep], st_send, st_recv, to_ep(d)).start()

    sin[ep] = sout[ep]

    streams = [(0, 1, NY // 2), (1, -1, NY // 2), (0, -1, NY // 2 - 1), (1, 1, NY // 2 - 1)]

    def lane(o, c):
        return lax.rem(y + o + NY, NY) * 2 + c

    def chunk(c):
        return pl.ds(c * HALF, HALF)

    def ring(k, i):
        c, s, _ = streams[k]
        t = lane(-s * i, core)
        blk = xall.at[t, chunk(c)]
        return rcopy(blk, blk, ag_send, ag_recv.at[k, i], to_y(s))

    def ring_recv(k, i):
        c, s, _ = streams[k]
        t = lane(-s * (i + 1), core)
        blk = xall.at[t, chunk(c)]
        return rcopy(blk, blk, ag_send, ag_recv.at[k, i], to_y(s))

    def cross(o, c):
        blk = xall.at[lane(o, core), chunk(c)]
        return rcopy(blk, blk, d2_send, d2_recv.at[o % NY, c], sibling)

    def cross_recv(o, c):
        blk = xall.at[lane(o, other), chunk(c)]
        return rcopy(blk, blk, d2_send, d2_recv.at[o % NY, c], sibling)

    def expand(o, first=False):
        for c in range(2):
            cross_recv(o, c).wait_recv()
        yy = lax.rem(y + o + NY, NY)
        rows = jnp.concatenate(
            [flat(xall[2 * yy]), flat(xall[2 * yy + 1])], axis=1
        )
        ks = pl.ds(pl.multiple_of(yy * 2 * LANES, 2 * LANES), 2 * LANES)
        for acc, w in ((gate_acc, wg_v), (up_acc, wu_v)):
            prod = mm(rows, w[ks, :])
            if first:
                acc[...] = prod
            else:
                acc[...] += prod

    wait_bytes(outbox.at[pl.ds(0, (EP - 1) * UC)], disp_recv)
    for k in range(4):
        if streams[k][2] > 0:
            ring(k, 0).start()
    for c in range(2):
        cross(0, c).start()
    loads[4].wait()
    loads[5].wait()

    def local_part():
        c_conv = conv(c_v[...], halo[pl.ds(VR + NSTATE, NSTATE), :], tapc_ref[gsel, :]).astype(BF16)
        cc_v[...] = c_conv
        gram = mm(bc_v[...], c_conv, (((0,), (0,)), ((), ())))
        diag = lax.broadcasted_iota(jnp.int32, (LANES, LANES), 0) <= lax.broadcasted_iota(
            jnp.int32, (LANES, LANES), 1
        )
        for h in range(HH):
            for j in range(NB):
                at = cum_v[h : h + 1, j * LANES : (j + 1) * LANES]
                pieces = []
                for i in range(j + 1):
                    gap = at - colv[i * LANES : (i + 1) * LANES, h : h + 1]
                    if i == j:
                        gap = jnp.where(diag, gap, -jnp.inf)
                    g = gram[i * LANES : (i + 1) * LANES, j * LANES : (j + 1) * LANES]
                    pieces.append((g * jnp.exp(gap)).astype(BF16))
                weights = jnp.concatenate(pieces, axis=0) if j else pieces[0]
                rows_h = pl.ds(h * HD, HD)
                yloc[rows_h, j * LANES : (j + 1) * LANES] = mm(
                    xs_v[rows_h, : (j + 1) * LANES], weights
                )

    def prefix_part():
        wait_bytes(sout.at[pl.ds(0, EP - 1)], st_recv)
        held = jnp.zeros((U, LANES), F32)
        for e in range(EP):
            hout[e] = held
            blk = sin[e].astype(F32)
            keep = jnp.exp(blk[U : U + 1] + blk[U + 1 : U + 2] + blk[U + 2 : U + 3])
            held = keep * held + blk[:U]

        @pl.loop(1, EP)
        def _(d):
            tgt = lax.rem(ep + d, EP)
            rcopy(hout.at[tgt], hin.at[ep], hb_send, hb_recv, to_ep(d)).start()

        hin[ep] = hout[ep]

    def final_part():
        loads[7].wait()
        wait_bytes(hout.at[pl.ds(0, EP - 1)], hb_recv)
        before = hin[...].reshape(VR, LANES).astype(BF16)
        tall = jnp.concatenate([hgain_ref[...], jnp.zeros((8 - VR // LANES, LANES), F32)], axis=0)
        gains = jnp.transpose(tall)
        for h in range(HH):
            rows_h = pl.ds(h * HD, HD)
            carried = mm(before[h * HD : (h + 1) * HD], cc_v[...]) * jnp.exp(cum_v[h : h + 1, :])
            z = z_v[rows_h, :].astype(F32)
            gated = (yloc[rows_h, :] + carried) * (z * jax.nn.sigmoid(z))
            scale = lax.rsqrt(jnp.mean(gated * gated, axis=0, keepdims=True) + HEAD_EPS)
            lo = h * HD % LANES
            gain = gains[lo : lo + HD, h * HD // LANES : h * HD // LANES + 1]
            mixed_ref[rows_h, :] = (gated * scale * gain).astype(BF16)

    fill_gather = {0: local_part, 1: prefix_part}
    for i in range(NY // 2):
        if i in fill_gather:
            fill_gather[i]()
        expand(i, first=(i == 0))
        if i:
            expand(-i)
        for k in range(4):
            c, s, n = streams[k]
            if i < n:
                ring_recv(k, i).wait_recv()
                if i + 1 < n:
                    ring(k, i + 1).start()
                cross(-s * (i + 1), c).start()
    expand(NY // 2)

    gate = gate_acc[...]
    hid[...] = (gate * jax.nn.sigmoid(gate) * up_acc[...]).astype(BF16)

    loads[6].wait()

    def swap(o):
        return rcopy(part.at[o % NY, other], sib.at[o % NY], ps_send, ps_recv.at[o % NY], sibling)

    def project(o):
        yy = lax.rem(y + o + NY, NY)
        cols = pl.ds(pl.multiple_of(yy * 2 * LANES, 2 * LANES), 2 * LANES)
        prod = mm(hid[...], wd_v[:, cols]).astype(BF16)
        put(part.at[o % NY, 0], prod[:, :LANES])
        put(part.at[o % NY, 1], prod[:, LANES:])
        swap(o).start()

    swapped = set()

    def pair_sum(o, c):
        if o % NY not in swapped:
            swap(o).wait_recv()
            swapped.add(o % NY)
        mine = flat(part[o % NY, core, chunk(c)]).astype(F32)
        return mine + flat(sib[o % NY, chunk(c)]).astype(F32)

    slots, count = {}, 0
    for k in range(4):
        for i in range(streams[k][2]):
            slots[k, i] = count
            count += 1

    def push(k, i):
        j = slots[k, i]
        return rcopy(tosend.at[j], arrived.at[j], rs_send, rs_recv.at[j], to_y(streams[k][1]))

    def came(k, i):
        push(k, i).wait_recv()
        return flat(arrived[slots[k, i]]).astype(F32)

    reach = NY // 2
    project(reach)
    if reach > 1:
        project(reach - 1)
        project(1 - reach)
    fill_scatter = {1: final_part}
    for i in range(reach):
        for k in range(4):
            c, s, n = streams[k]
            if i < n:
                value = pair_sum(s * (n - i), c)
                if i:
                    value = value + came(k, i - 1)
                put(tosend.at[slots[k, i]], value.astype(BF16))
                push(k, i).start()
        left = reach - 2 - i
        if left >= 0:
            project(left)
            if left:
                project(-left)
        if i in fill_scatter:
            fill_scatter[i]()
    if reach == 1:
        project(0)
    for c in range(2):
        value = pair_sum(0, c)
        for k in range(4):
            if streams[k][0] == c and streams[k][2] > 0:
                value = value + came(k, streams[k][2] - 1)
        put(rout.at[chunk(c)], value.astype(BF16))

    @pl.loop(1, EP)
    def _(d):
        tgt = lax.rem(ep + d, EP)
        rcopy(
            rout.at[pl.ds(tgt * UC, UC)], rin.at[pl.ds(ep * UC, UC)], rt_send, rt_recv, to_ep(d)
        ).start()

    rin[pl.ds(ep * UC, UC)] = rout[pl.ds(ep * UC, UC)]
    logit = logit_ref[...]
    w0 = jax.nn.sigmoid(logit[:, 0:1] - logit[:, 1:2])
    w1 = jax.nn.sigmoid(logit[:, 1:2] - logit[:, 0:1])

    wait_bytes(outbox.at[pl.ds(0, (EP - 1) * UC)], disp_send)
    for h in halos:
        h.wait_send()
    wait_bytes(sout.at[pl.ds(0, EP - 1)], st_send)
    wait_bytes(hout.at[pl.ds(0, EP - 1)], hb_send)
    wait_bytes(xall.at[pl.ds(0, NY - 1)], ag_send)
    wait_bytes(xall.at[pl.ds(0, NY)], d2_send)
    wait_bytes(sib, ps_send)
    wait_bytes(tosend, rs_send)

    wait_bytes(rout.at[pl.ds(0, (EP - 1) * UC)], rt_recv)
    back = flat(rin[...])
    mixed_rows = mm(pick[0], back) * w0 + mm(pick[1], back) * w1
    moe_ref[...] = jnp.transpose(mixed_rows).astype(BF16)
    wait_bytes(rout.at[pl.ds(0, (EP - 1) * UC)], rt_send)


def on_device(EP, TP, *args):
    (x_in, z_in, dt_raw, decay_rate, b_in, c_in, conv_x, conv_b, conv_c, head_gain,
     moe_rows, moe_gain, routes, route_logit, w_gate, w_up, w_down) = args
    tokens, features = moe_rows.shape
    CAP = 2 * tokens * routes.shape[1] // EP
    VR, L = x_in.shape
    HH = dt_raw.shape[0]
    FD = w_gate.shape[2]
    NY = TP // 2
    ROWS = EP * CAP
    U = VR // EP
    UR = -(-(U + 8) // 16) * 16
    cfg = dict(EP=EP, TP=TP, CAP=CAP, L=L, HH=HH)
    any_, vmem, smem = (pl.BlockSpec(memory_space=m) for m in (pl.ANY, pltpu.VMEM, pltpu.SMEM))
    dma = pltpu.SemaphoreType.DMA
    units = (ROWS // QUAD, QUAD, LANES)
    half = (ROWS // QUAD // 2, QUAD, LANES)
    hops = 2 * (NY // 2) + 2 * (NY // 2 - 1)
    scratch = [
        pltpu.VMEM((VR, L), BF16), pltpu.VMEM((VR, L), BF16),
        pltpu.VMEM((NSTATE, L), BF16), pltpu.VMEM((NSTATE, L), BF16),
        pltpu.VMEM((tokens, features), BF16),
        pltpu.VMEM((features, FD), BF16), pltpu.VMEM((features, FD), BF16), pltpu.VMEM((FD, features), BF16),
        pltpu.VMEM((VR + 2 * NSTATE, LANES), BF16),
        pltpu.VMEM((2, tokens, ROWS), BF16),
        pltpu.VMEM(units, BF16), pltpu.VMEM((TP,) + units, BF16),
        pltpu.VMEM((ROWS, FD), F32), pltpu.VMEM((ROWS, FD), F32), pltpu.VMEM((ROWS, FD), BF16),
        pltpu.VMEM((NY, 2) + units, BF16), pltpu.VMEM((NY,) + units, BF16),
        pltpu.VMEM((hops,) + half, BF16), pltpu.VMEM((hops,) + half, BF16),
        pltpu.VMEM(units, BF16), pltpu.VMEM(units, BF16),
        pltpu.VMEM((VR, L), BF16), pltpu.VMEM((NSTATE, L), BF16), pltpu.VMEM((NSTATE, L), BF16),
        pltpu.VMEM((8, L), F32), pltpu.VMEM((L, 8), F32), pltpu.VMEM((VR, L), F32),
        pltpu.VMEM((EP, UR, LANES), BF16), pltpu.VMEM((EP, UR, LANES), BF16),
        pltpu.VMEM((EP, U, LANES), F32), pltpu.VMEM((EP, U, LANES), F32),
        dma((8,)), dma((3,)), dma((3,)), dma, dma, dma, dma, dma, dma,
        dma, dma((4, NY // 2)), dma, dma((NY, 2)), dma, dma((NY,)), dma, dma((hops,)), dma, dma,
    ]
    return pl.pallas_call(
        functools.partial(kernel_body, cfg),
        name="mixer_and_experts",
        out_shape=(
            jax.ShapeDtypeStruct((VR, L), BF16),
            jax.ShapeDtypeStruct((features // TP, tokens), BF16),
        ),
        in_specs=[
            any_, any_, vmem, smem, any_, any_, vmem, vmem, vmem, vmem,
            any_, vmem, vmem, vmem, any_, any_, any_,
        ],
        out_specs=(vmem, vmem),
        scratch_shapes=scratch,
        compiler_params=pltpu.CompilerParams(
            collective_id=0, has_side_effects=True, vmem_limit_bytes=60 * 1024 * 1024
        ),
    )(
        x_in, z_in, dt_raw, decay_rate, b_in, c_in, conv_x, conv_b, conv_c,
        head_gain.reshape(VR // LANES, LANES), moe_rows, moe_gain.reshape(TP, features // TP),
        routes, route_logit, w_gate, w_up, w_down,
    )


def solution(mesh):
    EP, TP = mesh.shape["ep"], mesh.shape["tp"]
    in_specs = (
        P("tp", "ep"), P("tp", "ep"), P("tp", "ep"), P("tp"), P(None, "ep"), P(None, "ep"),
        P("tp", None), P(), P(), P("tp"), P("ep", None), P(), P("ep", None), P("ep", None),
        P("ep", None, "tp"), P("ep", None, "tp"), P("ep", "tp", None),
    )
    return jax.shard_map(
        functools.partial(on_device, EP, TP),
        mesh=mesh,
        in_specs=in_specs,
        out_specs=(P("tp", "ep"), P("tp", "ep")),
        check_vma=False,
    )
```

time: 195 us -> 88.5 us (0.45)
  blocking collectives: 84.4 us -> 0 us
  Pallas kernels: 0 us -> 72.9 us
  waiting for transfers between devices: 27.7 us -> 0 us
  starting transfers between devices: 19.8 us -> 0 us
  matrix products: 18.8 us -> 0 us
  between operations: 15.3 us -> 0.64 us
  other arithmetic: 10.7 us -> 0 us
    pallas_call x0 -> x1, Pallas kernels: none -> 72.9 us  [on_device(): pl.pallas_call(functools.partial(kernel_body, cfg), name='mixer_and_exper...]
    all_gather x3 -> x0, blocking collectives: 53.7 us -> none  [entering(): lax.all_gather(part.astype(kind), axis)]
    all_to_all x1 -> x0, blocking collectives: 23.2 us -> none  [experts_half(): lax.all_to_all(outbox.reshape(experts, capacity, col_width), EP, split_ax...]
    all_to_all x2 -> x0, waiting for transfers between devices: 19 us -> none  [the longest x1 10.1 us: sent_and_summed(): lax.all_to_all(tiles, axis, split_axis=0, concat_axis=0, tiled=True)]
    dot_general x15 -> x0, matrix products: 18.8 us -> none  [the longest x1 7.12 us: experts_half(): lax.dot_general(columns, hidden, (((0,), (1,)), ((), ())), preferred_elem...]
    all_to_all x2 -> x0, starting transfers between devices: 15.5 us -> none  [the longest x1 10.4 us: experts_half(): lax.all_to_all(expert_out, EP, split_axis=1, concat_axis=1, tiled=True)]
    unnamed x34 -> x10, local copies, waits for them, and re-layouts: 2.05 us -> 13.1 us
    all_gather x1 -> x0, waiting for transfers between devices: 8.67 us -> none  [experts_half(): part_rows = lax.all_gather(arrived, 'tp', axis=1, tiled=True)]
  transfers between devices with their start and end apart: 4 -> 0, of which waited for: 3 -> 0; matrix products, arithmetic and copies ran while one was open for 9% -> 0% of each run, Pallas kernels for 0% -> 0%
where the time goes in v1:
time: 88.5 us; the launch traced here: 88.2 us
  Pallas kernels  72.9 us (82%)
  local copies, waits for them, and re-layouts  14.6 us (16%)
    pallas_call x1, Pallas kernels, on_device(): pl.pallas_call(functools.partial(kernel_body, cfg), name='mixer_and_exper...  72.9 us
    unnamed x10, local copies, waits for them, and re-layouts  13.1 us

profile of v1, /device:TPU:6, one launch (start us, length us, event | category | flops | bytes accessed | tf_op | source)
XLA Modules:
  0.0 88.2 jit_solution(14006439331793082464)
XLA Ops:
  0.6 1.4 %copy.22.routes_ref = s32[160,2]{1,0:T(8,128)} copy(s32[160,2]{0,1:T(2,128)} %param.29) | data formatting | bytes 2560 | tf_op args[12]
  2.1 1.4 %copy.23.logit_ref = f32[160,2]{1,0:T(8,128)} copy(f32[160,2]{0,1:T(2,128)} %param.30) | data formatting | bytes 2560 | tf_op args[13]
  3.5 1.5 %copy.19.tapx_ref = f32[256,4]{1,0:T(8,128)} copy(f32[256,4]{0,1:T(4,128)} %param.23) | data formatting | bytes 8192 | tf_op args[6]
  4.9 1.5 %copy.20.tapb_ref = f32[256,4]{1,0:T(8,128)} copy(f32[256,4]{0,1:T(4,128)} %param.24) | data formatting | bytes 8192 | tf_op args[7]
  6.4 1.5 %copy.21.tapc_ref = f32[256,4]{1,0:T(8,128)} copy(f32[256,4]{0,1:T(4,128)} %param.25) | data formatting | bytes 8192 | tf_op args[8]
  7.9 0.0 copy-start
  7.9 2.6 %copy.24.wg_hbm = bf16[1,2048,320]{2,1,0:T(8,128)(2,1)} copy(bf16[1,2048,320]{1,2,0:T(8,128)(2,1)} %param.31) | data formatting | bytes 2621440 | tf_op args[14]
  10.5 0.0 copy-done
  10.5 1.6 %copy.25.wu_hbm = bf16[1,2048,320]{2,1,0:T(8,128)(2,1)} copy(bf16[1,2048,320]{1,2,0:T(8,128)(2,1)S(1)} %copy-done) | data formatting | bytes 2621440 | tf_op args[15]
  12.1 72.9 %mixer_and_experts.1 = (bf16[256,384]{1,0:T(8,128)(2,1)}, bf16[128,160]{1,0:T(8,128)(2,1)}) custom-call(bf16[256,384]{1,0:T(8,128)(2,1)} %x_hbm.1, bf16[256,384]{1,0:T(8,128)(2,1)} %z_hbm.1, f32[4,384]{1,0:T(4,128)} %dt_ref.1, f32[4]{0:T(128)} %rate_ref.1, bf16[256,384]{1,0:T(8,128)(2,1)} %b_hbm.1, bf16[256,384]{1,0:T(8,128)(2,1)} %c_hbm.1, ...), custom_call_target="tpu_custom_call" | custom-call | tf_op jit(solution)/shard_map/mixer_and_experts/pallas_call | solution.py:480
  85.0 1.6 %copy.26 = bf16[128,160]{0,1:T(8,128)(2,1)} copy(bf16[128,160]{1,0:T(8,128)(2,1)} %get-tuple-element.3) | data formatting | bytes 81920 | tf_op jit(solution)/shard_map/mixer_and_experts/pallas_call | solution.py:480
  86.5 1.6 %copy.28 = bf16[256,384]{1,0:T(8,128)(2,1)} copy(bf16[256,384]{1,0:T(8,128)(2,1)} %get-tuple-element.6) | data formatting | bytes 393216
Async XLA Ops:
  7.9 2.7 %copy-start = (bf16[1,2048,320]{1,2,0:T(8,128)(2,1)S(1)}, bf16[1,2048,320]{1,2,0:T(8,128)(2,1)}, u32[]{:S(2)}) copy-start(bf16[1,2048,320]{1,2,0:T(8,128)(2,1)} %param.32) | copy-start | bytes 3932164

commit v2 on v1

--- a/solution.py
+++ b/solution.py
@@ -25,13 +25,15 @@
 
 def kernel_body(
     cfg,
-    x_hbm, z_hbm, dt_ref, rate_ref, b_hbm, c_hbm, tapx_ref, tapb_ref, tapc_ref, hgain_ref,
-    rows_hbm, mgain_ref, routes_ref, logit_ref, wg_hbm, wu_hbm, wd_hbm,
+    x_hbm, z_hbm, dt_hbm, rate_hbm, b_hbm, c_hbm, tapx_hbm, tapb_hbm, tapc_hbm, hgain_hbm,
+    rows_hbm, mgain_hbm, routes_hbm, logit_hbm, wg_hbm, wu_hbm, wd_hbm,
+    mixed_hbm, moe_hbm,
+    dt_ref, rate_ref, tapx_ref, tapb_ref, tapc_ref, hgain_ref, mgain_ref, routes_ref, logit_ref,
     mixed_ref, moe_ref,
     x_v, z_v, b_v, c_v, rows_v, wg_v, wu_v, wd_v, halo, pick, outbox, xall,
     gate_acc, up_acc, hid, part, sib, tosend, arrived, rout, rin,
     xs_v, bc_v, cc_v, cum_v, colv, yloc, sout, sin, hout, hin,
-    load_sem, halo_send, halo_recv, disp_send, disp_recv, st_send, st_recv, hb_send, hb_recv,
+    load_sem, store_sem, halo_send, halo_recv, disp_send, disp_recv, st_send, st_recv, hb_send, hb_recv,
     ag_send, ag_recv, d2_send, d2_recv, ps_send, ps_recv, rs_send, rs_recv, rt_send, rt_recv,
 ):
     EP, TP, CAP, L, HH = cfg["EP"], cfg["TP"], cfg["CAP"], cfg["L"], cfg["HH"]
@@ -72,19 +74,6 @@
     def wait_bytes(ref, sem):
         pltpu.make_async_copy(ref, ref, sem).wait()
 
-    gsel = pl.ds(pl.multiple_of(group * NSTATE, NSTATE), NSTATE)
-    loads = [
-        pltpu.make_async_copy(src, dst, load_sem.at[i])
-        for i, (src, dst) in enumerate(
-            (
-                (rows_hbm, rows_v), (x_hbm, x_v), (b_hbm.at[gsel, :], b_v), (c_hbm.at[gsel, :], c_v),
-                (wg_hbm.at[0], wg_v), (wu_hbm.at[0], wu_v), (wd_hbm.at[0], wd_v), (z_hbm, z_v),
-            )
-        )
-    ]
-    for load in loads:
-        load.start()
-
     barrier = pltpu.get_barrier_semaphore()
 
     @pl.loop(1, EP)
@@ -94,33 +83,50 @@
     for dev in (to_y(1), to_y(-1), sibling):
         pl.semaphore_signal(barrier, inc=1, device_id=dev, device_id_type=MESH)
 
+    gsel = pl.ds(pl.multiple_of(group * NSTATE, NSTATE), NSTATE)
+    loads = {}
+    for i, (name, src, dst) in enumerate(
+        (
+            ("routes", routes_hbm, routes_ref), ("rows", rows_hbm, rows_v), ("mgain", mgain_hbm, mgain_ref),
+            ("logit", logit_hbm, logit_ref), ("dt", dt_hbm, dt_ref), ("rate", rate_hbm, rate_ref),
+            ("x", x_hbm, x_v), ("b", b_hbm.at[gsel, :], b_v), ("c", c_hbm.at[gsel, :], c_v),
+            ("tapx", tapx_hbm, tapx_ref), ("tapb", tapb_hbm, tapb_ref), ("tapc", tapc_hbm, tapc_ref),
+            ("hgain", hgain_hbm, hgain_ref),
+            ("wg", wg_hbm.at[0], wg_v), ("wu", wu_hbm.at[0], wu_v), ("wd", wd_hbm.at[0], wd_v),
+            ("z", z_hbm, z_v),
+        )
+    ):
+        loads[name] = pltpu.make_async_copy(src, dst, load_sem.at[i])
+        loads[name].start()
+
+    def ready(*names):
+        for name in names:
+            loads[name].wait()
+
+    ready("routes")
     routes = routes_ref[...]
-    lane_e = lax.broadcasted_iota(jnp.int32, (tokens, EP), 1)
-    hits = [(routes[:, k : k + 1] == lane_e).astype(F32) for k in range(2)]
-    below = (
+    row_e = lax.broadcasted_iota(jnp.int32, (EP, tokens), 0)
+    hits = [(routes[k : k + 1, :] == row_e).astype(F32) for k in range(2)]
+    before = (
         lax.broadcasted_iota(jnp.int32, (tokens, tokens), 0)
-        > lax.broadcasted_iota(jnp.int32, (tokens, tokens), 1)
+        < lax.broadcasted_iota(jnp.int32, (tokens, tokens), 1)
     ).astype(BF16)
-    ahead = mm(below, (hits[0] + hits[1]).astype(BF16))
-    lane_s = lax.broadcasted_iota(jnp.int32, (tokens, ROWS), 1)
-    onehot = None
+    ahead = mm((hits[0] + hits[1]).astype(BF16), before)
+    row_s = lax.broadcasted_iota(jnp.int32, (ROWS, tokens), 0)
+    hots = []
     for k in range(2):
-        rank = jnp.sum(ahead * hits[k], axis=1, keepdims=True).astype(jnp.int32)
-        slot = routes[:, k : k + 1] * CAP + rank
-        hot = (lane_s == slot).astype(F32)
-        pick[k] = hot.astype(BF16)
-        onehot = hot if onehot is None else onehot + hot
-
-    loads[0].wait()
+        rank = jnp.sum(ahead * hits[k], axis=0, keepdims=True).astype(jnp.int32)
+        hots.append(row_s == routes[k : k + 1, :] * CAP + rank)
+    onehot = (hots[0] | hots[1]).astype(F32).astype(BF16)
+
+    ready("rows", "mgain")
     rows_f = rows_v[...].astype(F32)
     row_scale = lax.rsqrt(jnp.mean(rows_f * rows_f, axis=1, keepdims=True) + ROW_EPS)
     own_cols = rows_v[:, pl.ds(pl.multiple_of(tp * LANES, LANES), LANES)].astype(F32)
     normed = (own_cols * row_scale * mgain_ref[pl.ds(tp, 1), :]).astype(BF16)
-    packed = mm(onehot.astype(BF16), normed, (((0,), (0,)), ((), ()))).astype(BF16)
+    packed = mm(onehot, normed).astype(BF16)
     put(outbox, packed)
 
-    for i in (1, 2, 3):
-        loads[i].wait()
     pl.semaphore_wait(barrier, EP - 1 + 3)
 
     @pl.loop(1, EP)
@@ -130,24 +136,21 @@
             outbox.at[pl.ds(tgt * UC, UC)], xall.at[tp, pl.ds(ep * UC, UC)], disp_send, disp_recv, to_ep(d)
         ).start()
 
-    last = pl.ds(L - LANES, LANES)
-    halos = [
-        rcopy(x_v.at[:, last], halo.at[pl.ds(0, VR)], halo_send.at[0], halo_recv.at[0], to_ep(1)),
-        rcopy(b_v.at[:, last], halo.at[pl.ds(VR, NSTATE)], halo_send.at[1], halo_recv.at[1], to_ep(1)),
-        rcopy(
-            c_v.at[:, last], halo.at[pl.ds(VR + NSTATE, NSTATE)], halo_send.at[2], halo_recv.at[2], to_ep(1)
-        ),
-    ]
-    for h in halos:
-        h.start()
     xall[tp, pl.ds(ep * UC, UC)] = outbox[pl.ds(ep * UC, UC)]
+
+    ready("logit", "dt", "rate")
+    logit = logit_ref[...]
+    share = jax.nn.sigmoid(logit[0:1, :] - logit[1:2, :])
+    weighted = jnp.where(hots[0], share, jnp.where(hots[1], jax.nn.sigmoid(logit[1:2, :] - logit[0:1, :]), 0.0))
+    weighted = jnp.transpose(weighted)
+    coarse = weighted.astype(BF16)
+    pick[0] = coarse
+    pick[1] = (weighted - coarse.astype(F32)).astype(BF16)
 
     dt = dt_ref[...]
     step = jnp.maximum(dt, 0.0) + jnp.log1p(jnp.exp(-jnp.abs(dt)))
-    head_row = lax.broadcasted_iota(jnp.int32, (HH, L), 0)
-    rate = jnp.zeros((HH, L), F32)
-    for h in range(HH):
-        rate = jnp.where(head_row == h, rate_ref[h], rate)
+    eye = lax.broadcasted_iota(jnp.int32, (HH, HH), 0) == lax.broadcasted_iota(jnp.int32, (HH, HH), 1)
+    rate = jnp.sum(jnp.where(eye, rate_ref[...], 0.0), axis=1, keepdims=True)
     logd = -step * rate
     upper = (
         lax.broadcasted_iota(jnp.int32, (LANES, LANES), 0)
@@ -169,55 +172,6 @@
     tall = jnp.concatenate([cum, jnp.zeros((8 - HH, L), F32)], axis=0)
     colv[...] = jnp.transpose(tall)
 
-    for h in halos:
-        h.wait_recv()
-    started = (ep > 0).astype(F32)
-
-    def conv(cur, rim, taps):
-        joined = jnp.concatenate([rim.astype(F32) * started, cur.astype(F32)], axis=1)
-        out = taps[:, 3:4] * joined[:, LANES:]
-        for k in range(3):
-            out = out + taps[:, k : k + 1] * pltpu.roll(joined, 3 - k, 1)[:, LANES:]
-        return out * jax.nn.sigmoid(out)
-
-    b_conv = conv(b_v[...], halo[pl.ds(VR, NSTATE), :], tapb_ref[gsel, :]).astype(BF16)
-    bc_v[...] = b_conv
-    tail = jnp.exp(total - cum)
-    for h in range(HH):
-        rows_h = pl.ds(h * HD, HD)
-        xc = conv(x_v[rows_h, :], halo[rows_h, :], tapx_ref[rows_h, :])
-        xs = xc * step[h : h + 1, :]
-        xs_v[rows_h, :] = xs.astype(BF16)
-        yloc[rows_h, :] = xs * tail[h : h + 1, :]
-    state = mm(yloc[...].astype(BF16), b_conv, (((1,), (1,)), ((), ())))
-
-    hi = total.astype(BF16).astype(F32)
-    mid = (total - hi).astype(BF16).astype(F32)
-    low = total - hi - mid
-    r8 = lax.broadcasted_iota(jnp.int32, (8, LANES), 0)
-    decays = []
-    for u in range(EP):
-        h = u * U // HD
-        decays.append(
-            jnp.where(
-                r8 == 0,
-                hi[h : h + 1],
-                jnp.where(r8 == 1, mid[h : h + 1], jnp.where(r8 == 2, low[h : h + 1], 0.0)),
-            )
-        )
-    for u in range(EP):
-        extra = [state[u * U : (u + 1) * U], decays[u]]
-        if UR > U + 8:
-            extra.append(jnp.zeros((UR - U - 8, LANES), F32))
-        sout[u] = jnp.concatenate(extra, axis=0).astype(BF16)
-
-    @pl.loop(1, EP)
-    def _(d):
-        tgt = lax.rem(ep + d, EP)
-        rcopy(sout.at[tgt], sin.at[ep], st_send, st_recv, to_ep(d)).start()
-
-    sin[ep] = sout[ep]
-
     streams = [(0, 1, NY // 2), (1, -1, NY // 2), (0, -1, NY // 2 - 1), (1, 1, NY // 2 - 1)]
 
     def lane(o, c):
@@ -255,7 +209,7 @@
         )
         ks = pl.ds(pl.multiple_of(yy * 2 * LANES, 2 * LANES), 2 * LANES)
         for acc, w in ((gate_acc, wg_v), (up_acc, wu_v)):
-            prod = mm(rows, w[ks, :])
+            prod = mm(rows, w[:, ks], (((1,), (1,)), ((), ())))
             if first:
                 acc[...] = prod
             else:
@@ -267,11 +221,78 @@
             ring(k, 0).start()
     for c in range(2):
         cross(0, c).start()
-    loads[4].wait()
-    loads[5].wait()
+    ready("x", "b", "c")
+    last = pl.ds(L - LANES, LANES)
+    halos = [
+        rcopy(x_v.at[:, last], halo.at[pl.ds(0, VR)], halo_send.at[0], halo_recv.at[0], to_ep(1)),
+        rcopy(b_v.at[:, last], halo.at[pl.ds(VR, NSTATE)], halo_send.at[1], halo_recv.at[1], to_ep(1)),
+        rcopy(
+            c_v.at[:, last], halo.at[pl.ds(VR + NSTATE, NSTATE)], halo_send.at[2], halo_recv.at[2], to_ep(1)
+        ),
+    ]
+    for h in halos:
+        h.start()
+    ready("wg", "wu")
+
+    started = (ep > 0).astype(F32)
+
+    def conv(cur, rim, taps):
+        joined = jnp.concatenate([rim.astype(F32) * started, cur.astype(F32)], axis=1)
+        out = taps[:, 3:4] * joined[:, LANES:]
+        for k in range(3):
+            out = out + taps[:, k : k + 1] * pltpu.roll(joined, 3 - k, 1)[:, LANES:]
+        return out * jax.nn.sigmoid(out)
+
+    def state_part():
+        for h in halos:
+            h.wait_recv()
+
+        ready("tapx", "tapb", "tapc", "hgain")
+        taps_bc = jnp.transpose(jnp.concatenate([tapb_ref[:, gsel], tapc_ref[:, gsel]], axis=0))
+        taps_x = jnp.transpose(
+            jnp.concatenate([tapx_ref[...], hgain_ref[...], jnp.zeros((3, VR), F32)], axis=0)
+        )
+        b_conv = conv(b_v[...], halo[pl.ds(VR, NSTATE), :], taps_bc[:, :4]).astype(BF16)
+        bc_v[...] = b_conv
+        tail = jnp.exp(total - cum)
+        for h in range(HH):
+            rows_h = pl.ds(h * HD, HD)
+            xc = conv(x_v[rows_h, :], halo[rows_h, :], taps_x[h * HD : (h + 1) * HD, :4])
+            xs = xc * step[h : h + 1, :]
+            xs_v[rows_h, :] = xs.astype(BF16)
+            yloc[rows_h, :] = xs * tail[h : h + 1, :]
+        state = mm(yloc[...].astype(BF16), b_conv, (((1,), (1,)), ((), ())))
+
+        hi = total.astype(BF16).astype(F32)
+        mid = (total - hi).astype(BF16).astype(F32)
+        low = total - hi - mid
+        r8 = lax.broadcasted_iota(jnp.int32, (8, LANES), 0)
+        decays = []
+        for u in range(EP):
+            h = u * U // HD
+            decays.append(
+                jnp.where(
+                    r8 == 0,
+                    hi[h : h + 1],
+                    jnp.where(r8 == 1, mid[h : h + 1], jnp.where(r8 == 2, low[h : h + 1], 0.0)),
+                )
+            )
+        for u in range(EP):
+            extra = [state[u * U : (u + 1) * U], decays[u]]
+            if UR > U + 8:
+                extra.append(jnp.zeros((UR - U - 8, LANES), F32))
+            sout[u] = jnp.concatenate(extra, axis=0).astype(BF16)
+
+        @pl.loop(1, EP)
+        def _(d):
+            tgt = lax.rem(ep + d, EP)
+            rcopy(sout.at[tgt], sin.at[ep], st_send, st_recv, to_ep(d)).start()
+
+        sin[ep] = sout[ep]
+        return taps_x, taps_bc
 
     def local_part():
-        c_conv = conv(c_v[...], halo[pl.ds(VR + NSTATE, NSTATE), :], tapc_ref[gsel, :]).astype(BF16)
+        c_conv = conv(c_v[...], halo[pl.ds(VR + NSTATE, NSTATE), :], taps[1][:, 4:]).astype(BF16)
         cc_v[...] = c_conv
         gram = mm(bc_v[...], c_conv, (((0,), (0,)), ((), ())))
         diag = lax.broadcasted_iota(jnp.int32, (LANES, LANES), 0) <= lax.broadcasted_iota(
@@ -310,22 +331,21 @@
         hin[ep] = hout[ep]
 
     def final_part():
-        loads[7].wait()
+        ready("z")
         wait_bytes(hout.at[pl.ds(0, EP - 1)], hb_recv)
         before = hin[...].reshape(VR, LANES).astype(BF16)
-        tall = jnp.concatenate([hgain_ref[...], jnp.zeros((8 - VR // LANES, LANES), F32)], axis=0)
-        gains = jnp.transpose(tall)
         for h in range(HH):
             rows_h = pl.ds(h * HD, HD)
             carried = mm(before[h * HD : (h + 1) * HD], cc_v[...]) * jnp.exp(cum_v[h : h + 1, :])
             z = z_v[rows_h, :].astype(F32)
             gated = (yloc[rows_h, :] + carried) * (z * jax.nn.sigmoid(z))
             scale = lax.rsqrt(jnp.mean(gated * gated, axis=0, keepdims=True) + HEAD_EPS)
-            lo = h * HD % LANES
-            gain = gains[lo : lo + HD, h * HD // LANES : h * HD // LANES + 1]
+            gain = taps[0][h * HD : (h + 1) * HD, 4:5]
             mixed_ref[rows_h, :] = (gated * scale * gain).astype(BF16)
 
-    fill_gather = {0: local_part, 1: prefix_part}
+    taps = []
+    early = 1 if NY > 4 else 0
+    fill_gather = {early: lambda: taps.extend(state_part()), early + 1: local_part}
     for i in range(NY // 2):
         if i in fill_gather:
             fill_gather[i]()
@@ -344,7 +364,7 @@
     gate = gate_acc[...]
     hid[...] = (gate * jax.nn.sigmoid(gate) * up_acc[...]).astype(BF16)
 
-    loads[6].wait()
+    ready("wd")
 
     def swap(o):
         return rcopy(part.at[o % NY, other], sib.at[o % NY], ps_send, ps_recv.at[o % NY], sibling)
@@ -384,11 +404,12 @@
     project(reach)
     if reach > 1:
         project(reach - 1)
-        project(1 - reach)
-    fill_scatter = {1: final_part}
+    fill_scatter = {min(1, reach - 1): prefix_part}
     for i in range(reach):
         for k in range(4):
             c, s, n = streams[k]
+            if i == 0 and k == 2 and reach > 1:
+                project(1 - reach)
             if i < n:
                 value = pair_sum(s * (n - i), c)
                 if i:
@@ -419,10 +440,12 @@
         ).start()
 
     rin[pl.ds(ep * UC, UC)] = rout[pl.ds(ep * UC, UC)]
-    logit = logit_ref[...]
-    w0 = jax.nn.sigmoid(logit[:, 0:1] - logit[:, 1:2])
-    w1 = jax.nn.sigmoid(logit[:, 1:2] - logit[:, 0:1])
-
+    final_part()
+    stores = [
+        pltpu.make_async_copy(mixed_ref, mixed_hbm, store_sem.at[0]),
+        pltpu.make_async_copy(moe_ref, moe_hbm, store_sem.at[1]),
+    ]
+    stores[0].start()
     wait_bytes(outbox.at[pl.ds(0, (EP - 1) * UC)], disp_send)
     for h in halos:
         h.wait_send()
@@ -435,9 +458,22 @@
 
     wait_bytes(rout.at[pl.ds(0, (EP - 1) * UC)], rt_recv)
     back = flat(rin[...])
-    mixed_rows = mm(pick[0], back) * w0 + mm(pick[1], back) * w1
-    moe_ref[...] = jnp.transpose(mixed_rows).astype(BF16)
+    moe_ref[...] = (mm(pick[0], back) + mm(pick[1], back)).astype(BF16)
+    stores[1].start()
+    for store in stores:
+        store.wait()
     wait_bytes(rout.at[pl.ds(0, (EP - 1) * UC)], rt_send)
+
+
+def place_body(mixed_ref, moe_ref, mixed_out, moe_out, sem):
+    copies = [
+        pltpu.make_async_copy(mixed_ref, mixed_out, sem.at[0]),
+        pltpu.make_async_copy(moe_ref, moe_out, sem.at[1]),
+    ]
+    for copy in copies:
+        copy.start()
+    for copy in copies:
+        copy.wait()
 
 
 def on_device(EP, TP, *args):
@@ -448,21 +484,27 @@
     VR, L = x_in.shape
     HH = dt_raw.shape[0]
     FD = w_gate.shape[2]
+    flipped = functools.partial(jnp.swapaxes, axis1=-2, axis2=-1)
     NY = TP // 2
     ROWS = EP * CAP
     U = VR // EP
     UR = -(-(U + 8) // 16) * 16
     cfg = dict(EP=EP, TP=TP, CAP=CAP, L=L, HH=HH)
-    any_, vmem, smem = (pl.BlockSpec(memory_space=m) for m in (pl.ANY, pltpu.VMEM, pltpu.SMEM))
+    hbm, vmem = (pl.BlockSpec(memory_space=m) for m in (pltpu.HBM, pltpu.VMEM))
     dma = pltpu.SemaphoreType.DMA
     units = (ROWS // QUAD, QUAD, LANES)
     half = (ROWS // QUAD // 2, QUAD, LANES)
     hops = 2 * (NY // 2) + 2 * (NY // 2 - 1)
     scratch = [
+        pltpu.VMEM((HH, L), F32), pltpu.VMEM((1, HH), F32),
+        pltpu.VMEM((4, VR), F32), pltpu.VMEM((4, conv_b.shape[0]), F32), pltpu.VMEM((4, conv_b.shape[0]), F32),
+        pltpu.VMEM((1, VR), F32), pltpu.VMEM((TP, features // TP), F32),
+        pltpu.VMEM((2, tokens), jnp.int32), pltpu.VMEM((2, tokens), F32),
+        pltpu.VMEM((VR, L), BF16), pltpu.VMEM((tokens, features // TP), BF16),
         pltpu.VMEM((VR, L), BF16), pltpu.VMEM((VR, L), BF16),
         pltpu.VMEM((NSTATE, L), BF16), pltpu.VMEM((NSTATE, L), BF16),
         pltpu.VMEM((tokens, features), BF16),
-        pltpu.VMEM((features, FD), BF16), pltpu.VMEM((features, FD), BF16), pltpu.VMEM((FD, features), BF16),
+        pltpu.VMEM((FD, features), BF16), pltpu.VMEM((FD, features), BF16), pltpu.VMEM((FD, features), BF16),
         pltpu.VMEM((VR + 2 * NSTATE, LANES), BF16),
         pltpu.VMEM((2, tokens, ROWS), BF16),
         pltpu.VMEM(units, BF16), pltpu.VMEM((TP,) + units, BF16),
@@ -474,30 +516,36 @@
         pltpu.VMEM((8, L), F32), pltpu.VMEM((L, 8), F32), pltpu.VMEM((VR, L), F32),
         pltpu.VMEM((EP, UR, LANES), BF16), pltpu.VMEM((EP, UR, LANES), BF16),
         pltpu.VMEM((EP, U, LANES), F32), pltpu.VMEM((EP, U, LANES), F32),
-        dma((8,)), dma((3,)), dma((3,)), dma, dma, dma, dma, dma, dma,
+        dma((17,)), dma((2,)), dma((3,)), dma((3,)), dma, dma, dma, dma, dma, dma,
         dma, dma((4, NY // 2)), dma, dma((NY, 2)), dma, dma((NY,)), dma, dma((hops,)), dma, dma,
     ]
-    return pl.pallas_call(
+    outs = pl.pallas_call(
         functools.partial(kernel_body, cfg),
         name="mixer_and_experts",
         out_shape=(
             jax.ShapeDtypeStruct((VR, L), BF16),
-            jax.ShapeDtypeStruct((features // TP, tokens), BF16),
+            jax.ShapeDtypeStruct((tokens, features // TP), BF16),
         ),
-        in_specs=[
-            any_, any_, vmem, smem, any_, any_, vmem, vmem, vmem, vmem,
-            any_, vmem, vmem, vmem, any_, any_, any_,
-        ],
-        out_specs=(vmem, vmem),
+        in_specs=[hbm] * 17,
+        out_specs=(hbm, hbm),
         scratch_shapes=scratch,
         compiler_params=pltpu.CompilerParams(
             collective_id=0, has_side_effects=True, vmem_limit_bytes=60 * 1024 * 1024
         ),
     )(
-        x_in, z_in, dt_raw, decay_rate, b_in, c_in, conv_x, conv_b, conv_c,
-        head_gain.reshape(VR // LANES, LANES), moe_rows, moe_gain.reshape(TP, features // TP),
-        routes, route_logit, w_gate, w_up, w_down,
+        x_in, z_in, dt_raw, decay_rate.reshape(1, HH), b_in, c_in, flipped(conv_x), flipped(conv_b), flipped(conv_c),
+        head_gain.reshape(1, VR), moe_rows, moe_gain.reshape(TP, features // TP),
+        flipped(routes), flipped(route_logit), flipped(w_gate), flipped(w_up), w_down,
     )
+    mixed, moe = pl.pallas_call(
+        place_body,
+        name="place",
+        out_shape=tuple(jax.ShapeDtypeStruct(o.shape, o.dtype) for o in outs),
+        in_specs=[vmem, vmem],
+        out_specs=(hbm, hbm),
+        scratch_shapes=[dma((2,))],
+    )(*outs)
+    return mixed, flipped(moe)
 
 
 def solution(mesh):

time: 88.5 us -> 70.5 us (0.80)
  the two profiles are of different devices: /device:TPU:6 before, /device:TPU:8 now
where the time goes in v2:
time: 70.5 us; the launch traced here: 70.4 us
  Pallas kernels  69.7 us (99%)
    pallas_call x1, Pallas kernels, on_device(): pl.pallas_call(functools.partial(kernel_body, cfg), name='mixer_and_exper...  68.1 us
    pallas_call x1, Pallas kernels, on_device(): pl.pallas_call(place_body, name='place', out_shape=tuple((jax.ShapeDtypeS...  1.63 us

profile of v2, /device:TPU:8, one launch (start us, length us, event | category | flops | bytes accessed | tf_op | source)
XLA Modules:
  0.0 70.4 jit_solution(11209233623320403749)
XLA Ops:
  0.6 68.1 %mixer_and_experts.1 = (bf16[256,384]{1,0:T(8,128)(2,1)}, bf16[160,128]{1,0:T(8,128)(2,1)}) custom-call(bf16[256,384]{1,0:T(8,128)(2,1)} %x_hbm.1, bf16[256,384]{1,0:T(8,128)(2,1)} %z_hbm.1, f32[4,384]{1,0:T(4,128)} %dt_hbm.1, f32[1,4]{1,0:T(1,128)} %bitcast.20, bf16[256,384]{1,0:T(8,128)(2,1)} %b_hbm.1, bf16[256,384]{1,0:T(8,128)(2,1)} %c_hbm.1, ...), custom_call_target="tpu_custom_call" | custom-call | tf_op jit(solution)/shard_map/mixer_and_experts/pallas_call | solution.py:522
  68.8 1.6 %place.1 = (bf16[256,384]{1,0:T(8,128)(2,1)}, bf16[160,128]{1,0:T(8,128)(2,1)}) custom-call(bf16[256,384]{1,0:T(8,128)(2,1)} %get-tuple-element.6.mixed_ref, bf16[160,128]{1,0:T(8,128)(2,1)} %get-tuple-element.7.moe_ref), custom_call_target="tpu_custom_call" | custom-call | tf_op jit(solution)/shard_map/place/pallas_call | solution.py:540

commit v3 on v2

v3 whole, which is shorter than its diff:
```python
import functools

import jax
import jax.numpy as jnp
from jax import lax
from jax.experimental import pallas as pl
from jax.experimental.pallas import tpu as pltpu
from jax.sharding import PartitionSpec as P

F32 = jnp.float32
BF16 = jnp.bfloat16
MESH = pl.DeviceIdType.MESH
HIGHEST = lax.Precision.HIGHEST
GROUPS = 2
NSTATE = 128
LANES = 128
QUAD = 4
ROW_EPS = 0.1
HEAD_EPS = 1.0


def mm(a, b, dims=(((1,), (0,)), ((), ()))):
    return lax.dot_general(a, b, dims, preferred_element_type=F32)


def kernel_body(
    cfg,
    x_hbm, z_hbm, dt_hbm, rate_hbm, b_hbm, c_hbm, tapx_hbm, tapb_hbm, tapc_hbm, hgain_hbm,
    rows_hbm, mgain_hbm, routes_hbm, logit_hbm, wg_hbm, wu_hbm, wd_hbm,
    mixed_ref, moe_ref,
    dt_ref, rate_ref, tapx_ref, tapb_ref, tapc_ref, hgain_ref, mgain_ref, routes_ref, logit_ref,
    x_v, z_v, b_v, c_v, rows_v, wg_v, wu_v, wd_v, halo, pick, outbox, inbox, xall,
    gate_acc, up_acc, hid, part, sib, tosend, arrived, rout, rin,
    xs_v, bc_v, cc_v, gram_v, cum_v, colv, yloc, sout, sin, hout, hin,
    load_sem, halo_send, halo_recv, disp_send, disp_recv, st_send, st_recv, hb_send, hb_recv,
    ag_send, ag_recv, d2_send, d2_recv, ps_send, ps_recv, rs_send, rs_recv, rt_send, rt_recv,
):
    EP, TP, CAP, L, HH = cfg["EP"], cfg["TP"], cfg["CAP"], cfg["L"], cfg["HH"]
    NY = TP // 2
    UC = CAP // QUAD
    ROWS = EP * CAP
    half_rows, quarter = ROWS // 2, ROWS // 4
    tokens = rows_v.shape[0]
    VR = x_v.shape[0]
    HD = VR // HH
    NB = L // LANES
    U = VR // EP
    UR = sout.shape[1]
    ep, tp = lax.axis_index("ep"), lax.axis_index("tp")
    y, core = lax.div(tp, 2), lax.rem(tp, 2)
    other = 1 - core
    group = lax.div(tp, TP // GROUPS)

    NX = min(4, EP)
    NZ = EP // NX
    z_at, x_at = lax.div(ep, NX), lax.rem(ep, NX)

    def hops(offset):
        dz, dx = offset
        return min(dz, NZ - dz) + min(dx, NX - dx)

    offsets = sorted(((dz, dx) for dz in range(NZ) for dx in range(NX) if dz or dx), key=lambda o: -hops(o))
    partners = [lax.rem(z_at + dz, NZ) * NX + lax.rem(x_at + dx, NX) for dz, dx in offsets]

    def at_ep(index):
        return {"ep": index, "tp": tp}

    def to_y(s):
        return {"ep": ep, "tp": lax.rem(y + s + NY, NY) * 2 + core}

    sibling = {"ep": ep, "tp": y * 2 + other}

    def rcopy(src, dst, ssem, rsem, dev):
        return pltpu.make_async_remote_copy(
            src_ref=src, dst_ref=dst, send_sem=ssem, recv_sem=rsem, device_id=dev, device_id_type=MESH
        )

    def flat(block):
        return block.reshape(block.shape[0] * QUAD, LANES)

    def put(ref, value):
        ref[...] = value.reshape(value.shape[0] // QUAD, QUAD, LANES)

    def wait_bytes(ref, sem):
        pltpu.make_async_copy(ref, ref, sem).wait()

    barrier = pltpu.get_barrier_semaphore()

    for tgt in partners:
        pl.semaphore_signal(barrier, inc=1, device_id=at_ep(tgt), device_id_type=MESH)

    for dev in (to_y(1), to_y(-1), sibling):
        pl.semaphore_signal(barrier, inc=1, device_id=dev, device_id_type=MESH)

    gsel = pl.ds(pl.multiple_of(group * NSTATE, NSTATE), NSTATE)
    loads = {}
    for i, (name, src, dst) in enumerate(
        (
            ("routes", routes_hbm, routes_ref), ("rows", rows_hbm, rows_v), ("mgain", mgain_hbm, mgain_ref),
            ("logit", logit_hbm, logit_ref), ("dt", dt_hbm, dt_ref), ("rate", rate_hbm, rate_ref),
            ("x", x_hbm, x_v), ("b", b_hbm.at[gsel, :], b_v), ("c", c_hbm.at[gsel, :], c_v),
            ("tapx", tapx_hbm, tapx_ref), ("tapb", tapb_hbm, tapb_ref), ("tapc", tapc_hbm, tapc_ref),
            ("hgain", hgain_hbm, hgain_ref),
            ("wg", wg_hbm.at[0], wg_v), ("wu", wu_hbm.at[0], wu_v), ("wd", wd_hbm.at[0], wd_v),
            ("z", z_hbm, z_v),
        )
    ):
        loads[name] = pltpu.make_async_copy(src, dst, load_sem.at[i])
        loads[name].start()

    def ready(*names):
        for name in names:
            loads[name].wait()

    ready("routes")
    routes = routes_ref[...]
    row_e = lax.broadcasted_iota(jnp.int32, (EP, tokens), 0)
    hits = [(routes[k : k + 1, :] == row_e).astype(F32) for k in range(2)]
    before = (
        lax.broadcasted_iota(jnp.int32, (tokens, tokens), 0)
        < lax.broadcasted_iota(jnp.int32, (tokens, tokens), 1)
    ).astype(BF16)
    ahead = mm((hits[0] + hits[1]).astype(BF16), before)
    row_s = lax.broadcasted_iota(jnp.int32, (ROWS, tokens), 0)
    hots = []
    for k in range(2):
        rank = jnp.sum(ahead * hits[k], axis=0, keepdims=True).astype(jnp.int32)
        hots.append(row_s == routes[k : k + 1, :] * CAP + rank)
    onehot = (hots[0] | hots[1]).astype(F32).astype(BF16)

    ready("rows", "mgain")
    rows_f = rows_v[...].astype(F32)
    row_scale = lax.rsqrt(jnp.mean(rows_f * rows_f, axis=1, keepdims=True) + ROW_EPS)
    own_cols = rows_v[:, pl.ds(pl.multiple_of(tp * LANES, LANES), LANES)].astype(F32)
    normed = (own_cols * row_scale * mgain_ref[pl.ds(tp, 1), :]).astype(BF16)
    packed = mm(onehot, normed).astype(BF16)
    put(outbox, packed)

    pl.semaphore_wait(barrier, EP - 1 + 3)

    for tgt in partners:
        rcopy(
            outbox.at[pl.ds(tgt * UC, UC)], inbox.at[pl.ds(ep * UC, UC)], disp_send, disp_recv, at_ep(tgt)
        ).start()

    inbox[pl.ds(ep * UC, UC)] = outbox[pl.ds(ep * UC, UC)]

    ready("logit", "dt", "rate")
    logit = logit_ref[...]
    share = jax.nn.sigmoid(logit[0:1, :] - logit[1:2, :])
    weighted = jnp.where(hots[0], share, jnp.where(hots[1], jax.nn.sigmoid(logit[1:2, :] - logit[0:1, :]), 0.0))
    weighted = jnp.transpose(weighted)
    coarse = weighted.astype(BF16)
    pick[0] = coarse
    pick[1] = (weighted - coarse.astype(F32)).astype(BF16)

    dt = dt_ref[...]
    step = jnp.maximum(dt, 0.0) + jnp.log1p(jnp.exp(-jnp.abs(dt)))
    eye = lax.broadcasted_iota(jnp.int32, (HH, HH), 0) == lax.broadcasted_iota(jnp.int32, (HH, HH), 1)
    rate = jnp.sum(jnp.where(eye, rate_ref[...], 0.0), axis=1, keepdims=True)
    logd = -step * rate
    upper = (
        lax.broadcasted_iota(jnp.int32, (LANES, LANES), 0)
        <= lax.broadcasted_iota(jnp.int32, (LANES, LANES), 1)
    ).astype(F32)
    pieces, carry = [], jnp.zeros((HH, 1), F32)
    for k in range(NB):
        piece = (
            jnp.dot(
                logd[:, k * LANES : (k + 1) * LANES], upper, precision=HIGHEST, preferred_element_type=F32
            )
            + carry
        )
        carry = piece[:, LANES - 1 : LANES]
        pieces.append(piece)
    cum = jnp.concatenate(pieces, axis=1)
    total = carry
    cum_v[pl.ds(0, HH), :] = cum
    tall = jnp.concatenate([cum, jnp.zeros((8 - HH, L), F32)], axis=0)
    colv[...] = jnp.transpose(tall)

    reach = NY // 2
    streams = []
    for q in range(4):
        streams.append((q, 1, reach - q % 2))
        streams.append((q, -1, reach - 1 + q % 2))

    def lane(o, c):
        return lax.rem(y + o + NY, NY) * 2 + c

    def part_of(q):
        return pl.ds(q * quarter, quarter)

    def half_of(h):
        return pl.ds(h * half_rows, half_rows)

    phases = ((0, 3), (4, 7), (1, 2), (5, 6))
    slots, count = {}, 0
    for k in range(8):
        for i in range(streams[k][2]):
            slots[k, i] = count
            count += 1

    def live(p, i):
        return [k for k in phases[p] if i < streams[k][2]]

    def ring(k, i):
        q, s, _ = streams[k]
        blk = xall.at[lane(-s * i, core), part_of(q)]
        return rcopy(blk, blk, ag_send, ag_recv.at[slots[k, i]], to_y(s))

    def ring_recv(k, i):
        q, s, _ = streams[k]
        blk = xall.at[lane(-s * (i + 1), core), part_of(q)]
        return rcopy(blk, blk, ag_send, ag_recv.at[slots[k, i]], to_y(s))

    def cross(o, q):
        blk = xall.at[lane(o, core), part_of(q)]
        return rcopy(blk, blk, d2_send, d2_recv.at[o % NY, q // 2], sibling)

    def cross_half(o, h, c):
        blk = xall.at[lane(o, c), half_of(h)]
        return rcopy(blk, blk, d2_send, d2_recv.at[o % NY, h], sibling)

    def drain(i, p):
        for k in live(p, i):
            q, s, n = streams[k]
            ring_recv(k, i).wait_recv()
            if i + 1 < n:
                ring(k, i + 1).start()
            cross(-s * (i + 1), q).start()

    def expand(o, h, first=False):
        cross_half(o, h, other).wait_recv()
        yy = lax.rem(y + o + NY, NY)
        rows = jnp.concatenate([xall[2 * yy, half_of(h), :], xall[2 * yy + 1, half_of(h), :]], axis=1)
        ks = pl.ds(pl.multiple_of(yy * 2 * LANES, 2 * LANES), 2 * LANES)
        for acc, w in ((gate_acc, wg_v), (up_acc, wu_v)):
            prod = mm(rows, w[:, ks], (((1,), (1,)), ((), ())))
            if first:
                acc[half_of(h), :] = prod
            else:
                acc[half_of(h), :] += prod

    wait_bytes(outbox.at[pl.ds(0, (EP - 1) * UC)], disp_recv)
    xall[tp] = flat(inbox[...])
    for p in range(4):
        for k in live(p, 0):
            ring(k, 0).start()
    for h in range(2):
        cross_half(0, h, core).start()
    ready("x", "b", "c")
    last = pl.ds(L - LANES, LANES)
    halos = [
        rcopy(x_v.at[:, last], halo.at[pl.ds(0, VR)], halo_send.at[0], halo_recv.at[0], at_ep(lax.rem(ep + 1, EP))),
        rcopy(b_v.at[:, last], halo.at[pl.ds(VR, NSTATE)], halo_send.at[1], halo_recv.at[1], at_ep(lax.rem(ep + 1, EP))),
        rcopy(
            c_v.at[:, last], halo.at[pl.ds(VR + NSTATE, NSTATE)], halo_send.at[2], halo_recv.at[2], at_ep(lax.rem(ep + 1, EP))
        ),
    ]
    for h in halos:
        h.start()
    ready("wg", "wu")

    started = (ep > 0).astype(F32)

    def conv(cur, rim, taps):
        joined = jnp.concatenate([rim.astype(F32) * started, cur.astype(F32)], axis=1)
        out = taps[:, 3:4] * joined[:, LANES:]
        for k in range(3):
            out = out + taps[:, k : k + 1] * pltpu.roll(joined, 3 - k, 1)[:, LANES:]
        return out * jax.nn.sigmoid(out)

    kept = {}

    def taps_part():
        for h in halos:
            h.wait_recv()
        ready("tapx", "tapb", "tapc", "hgain")
        kept["bc"] = jnp.transpose(jnp.concatenate([tapb_ref[:, gsel], tapc_ref[:, gsel]], axis=0))
        kept["x"] = jnp.transpose(
            jnp.concatenate([tapx_ref[...], hgain_ref[...], jnp.zeros((3, VR), F32)], axis=0)
        )
        bc_v[...] = conv(b_v[...], halo[pl.ds(VR, NSTATE), :], kept["bc"][:, :4]).astype(BF16)

    def value_part(heads):
        tail = jnp.exp(total - cum)
        for h in heads:
            rows_h = pl.ds(h * HD, HD)
            xc = conv(x_v[rows_h, :], halo[rows_h, :], kept["x"][h * HD : (h + 1) * HD, :4])
            xs = xc * step[h : h + 1, :]
            xs_v[rows_h, :] = xs.astype(BF16)
            yloc[rows_h, :] = xs * tail[h : h + 1, :]

    def send_part():
        state = mm(yloc[...].astype(BF16), bc_v[...], (((1,), (1,)), ((), ())))
        hi = total.astype(BF16).astype(F32)
        mid = (total - hi).astype(BF16).astype(F32)
        low = total - hi - mid
        r8 = lax.broadcasted_iota(jnp.int32, (8, LANES), 0)
        for u in range(EP):
            h = u * U // HD
            decay = jnp.where(
                r8 == 0,
                hi[h : h + 1],
                jnp.where(r8 == 1, mid[h : h + 1], jnp.where(r8 == 2, low[h : h + 1], 0.0)),
            )
            extra = [state[u * U : (u + 1) * U], decay]
            if UR > U + 8:
                extra.append(jnp.zeros((UR - U - 8, LANES), F32))
            sout[u] = jnp.concatenate(extra, axis=0).astype(BF16)

        @pl.loop(1, EP)
        def _(d):
            tgt = lax.rem(ep + d, EP)
            rcopy(sout.at[tgt], sin.at[ep], st_send, st_recv, at_ep(tgt)).start()

        sin[ep] = sout[ep]

    def gram_part():
        c_conv = conv(c_v[...], halo[pl.ds(VR + NSTATE, NSTATE), :], kept["bc"][:, 4:]).astype(BF16)
        cc_v[...] = c_conv
        gram_v[...] = mm(bc_v[...], c_conv, (((0,), (0,)), ((), ())))

    def local_part(heads):
        diag = lax.broadcasted_iota(jnp.int32, (LANES, LANES), 0) <= lax.broadcasted_iota(
            jnp.int32, (LANES, LANES), 1
        )
        for h in heads:
            for j in range(NB):
                at = cum_v[h : h + 1, j * LANES : (j + 1) * LANES]
                pieces = []
                for i in range(j + 1):
                    gap = at - colv[i * LANES : (i + 1) * LANES, h : h + 1]
                    if i == j:
                        gap = jnp.where(diag, gap, -jnp.inf)
                    g = gram_v[i * LANES : (i + 1) * LANES, j * LANES : (j + 1) * LANES]
                    pieces.append((g * jnp.exp(gap)).astype(BF16))
                weights = jnp.concatenate(pieces, axis=0) if j else pieces[0]
                rows_h = pl.ds(h * HD, HD)
                yloc[rows_h, j * LANES : (j + 1) * LANES] = mm(
                    xs_v[rows_h, : (j + 1) * LANES], weights
                )

    def prefix_part():
        wait_bytes(sout.at[pl.ds(0, EP - 1)], st_recv)
        held = jnp.zeros((U, LANES), F32)
        for e in range(EP):
            hout[e] = held
            blk = sin[e].astype(F32)
            keep = jnp.exp(blk[U : U + 1] + blk[U + 1 : U + 2] + blk[U + 2 : U + 3])
            held = keep * held + blk[:U]

        @pl.loop(1, EP)
        def _(d):
            tgt = lax.rem(ep + d, EP)
            rcopy(hout.at[tgt], hin.at[ep], hb_send, hb_recv, at_ep(tgt)).start()

        hin[ep] = hout[ep]

    def final_part():
        ready("z")
        wait_bytes(hout.at[pl.ds(0, EP - 1)], hb_recv)
        before = hin[...].reshape(VR, LANES).astype(BF16)
        for h in range(HH):
            rows_h = pl.ds(h * HD, HD)
            carried = mm(before[h * HD : (h + 1) * HD], cc_v[...]) * jnp.exp(cum_v[h : h + 1, :])
            z = z_v[rows_h, :].astype(F32)
            gated = (yloc[rows_h, :] + carried) * (z * jax.nn.sigmoid(z))
            scale = lax.rsqrt(jnp.mean(gated * gated, axis=0, keepdims=True) + HEAD_EPS)
            gain = kept["x"][h * HD : (h + 1) * HD, 4:5]
            mixed_ref[rows_h, :] = (gated * scale * gain).astype(BF16)

    pieces = [
        taps_part,
        lambda: value_part(range(HH // 2)),
        lambda: value_part(range(HH // 2, HH)),
        send_part,
        gram_part,
        lambda: local_part([0]),
        lambda: local_part([1]),
        lambda: local_part(range(2, HH)),
    ]

    for h in range(2):
        expand(0, h, first=True)
    far = reach - 1
    for i in range(far):
        for p in range(4):
            drain(i, p)
            if i:
                expand((i, -i, i, -i)[p], p // 2)
            if (i or p > 1) and pieces:
                pieces.pop(0)()
    if far:
        expand(far, 0)
    for piece in pieces:
        piece()
    drain(far, 0)
    if far:
        expand(-far, 0)
    drain(far, 1)
    if far:
        expand(far, 1)
        expand(-far, 1)

    ready("wd")

    def activate(h):
        gate = gate_acc[half_of(h), :]
        hid[half_of(h), :] = (gate * jax.nn.sigmoid(gate) * up_acc[half_of(h), :]).astype(BF16)

    def swap(o, h):
        return rcopy(
            part.at[o % NY, other, half_of(h)], sib.at[o % NY, half_of(h)], ps_send, ps_recv.at[o % NY, h], sibling
        )

    def project(o, h):
        yy = lax.rem(y + o + NY, NY)
        cols = pl.ds(pl.multiple_of(yy * 2 * LANES, 2 * LANES), 2 * LANES)
        prod = mm(hid[half_of(h), :], wd_v[:, cols]).astype(BF16)
        part[o % NY, 0, half_of(h), :] = prod[:, :LANES]
        part[o % NY, 1, half_of(h), :] = prod[:, LANES:]
        swap(o, h).start()

    swapped = set()

    def pair_sum(o, q):
        at = (o % NY, q // 2)
        if at not in swapped:
            swap(*at).wait_recv()
            swapped.add(at)
        mine = part[o % NY, core, part_of(q), :].astype(F32)
        return mine + sib[o % NY, part_of(q), :].astype(F32)

    def push(k, i):
        j = slots[k, i]
        return rcopy(tosend.at[j], arrived.at[j], rs_send, rs_recv.at[j], to_y(streams[k][1]))

    def came(k, i):
        push(k, i).wait_recv()
        return arrived[slots[k, i]].astype(F32)

    def feed(k, i):
        q, s, n = streams[k]
        value = pair_sum(s * (n - i), q)
        if i:
            value = value + came(k, i - 1)
        tosend[slots[k, i]] = value.astype(BF16)
        push(k, i).start()

    def feed_all(p, i):
        for k in live(p, i):
            feed(k, i)

    def project_for(i, side, h):
        m = reach - 1 - i
        if m > 0:
            project(side * m, h)
        elif m == 0 and side < 0:
            project(0, h)

    for h in range(2):
        expand(reach, h)
        activate(h)
        project(reach, h)
    feed_all(0, 0)
    project_for(0, -1, 0)
    feed_all(1, 0)
    project_for(0, 1, 0)
    project_for(0, -1, 1)
    project_for(0, 1, 1)
    feed_all(2, 0)
    project_for(1, -1, 0)
    feed_all(3, 0)
    project_for(1, 1, 0)
    for i in range(1, reach):
        for p in range(4):
            feed_all(p, i)
            if p < 2:
                project_for(i, (-1, 1)[p], 1)
            else:
                project_for(i + 1, (-1, 1)[p - 2], 0)
            if (i, p) == (min(2, far), 1):
                prefix_part()
    if reach == 1:
        project(0, 1)
    units = quarter // QUAD
    for q in range(4):
        value = pair_sum(0, q)
        for k in (2 * q, 2 * q + 1):
            if streams[k][2] > 0:
                value = value + came(k, streams[k][2] - 1)
        put(rout.at[pl.ds(q * units, units)], value.astype(BF16))

    for tgt in partners:
        rcopy(
            rout.at[pl.ds(tgt * UC, UC)], rin.at[pl.ds(ep * UC, UC)], rt_send, rt_recv, at_ep(tgt)
        ).start()

    rin[pl.ds(ep * UC, UC)] = rout[pl.ds(ep * UC, UC)]
    final_part()
    wait_bytes(outbox.at[pl.ds(0, (EP - 1) * UC)], disp_send)
    for h in halos:
        h.wait_send()
    wait_bytes(sout.at[pl.ds(0, EP - 1)], st_send)
    wait_bytes(hout.at[pl.ds(0, EP - 1)], hb_send)
    wait_bytes(xall.at[pl.ds(0, NY - 1)], ag_send)
    wait_bytes(xall.at[pl.ds(0, NY)], d2_send)
    wait_bytes(sib, ps_send)
    wait_bytes(tosend, rs_send)

    wait_bytes(rout.at[pl.ds(0, (EP - 1) * UC)], rt_recv)
    back = flat(rin[...])
    moe_ref[...] = (mm(pick[0], back) + mm(pick[1], back)).astype(BF16)
    wait_bytes(rout.at[pl.ds(0, (EP - 1) * UC)], rt_send)


def on_device(EP, TP, *args):
    (x_in, z_in, dt_raw, decay_rate, b_in, c_in, conv_x, conv_b, conv_c, head_gain,
     moe_rows, moe_gain, routes, route_logit, w_gate, w_up, w_down) = args
    tokens, features = moe_rows.shape
    CAP = 2 * tokens * routes.shape[1] // EP
    VR, L = x_in.shape
    HH = dt_raw.shape[0]
    FD = w_gate.shape[2]
    flipped = functools.partial(jnp.swapaxes, axis1=-2, axis2=-1)
    NY = TP // 2
    ROWS = EP * CAP
    U = VR // EP
    UR = -(-(U + 8) // 16) * 16
    cfg = dict(EP=EP, TP=TP, CAP=CAP, L=L, HH=HH)
    hbm, vmem = (pl.BlockSpec(memory_space=m) for m in (pltpu.HBM, pltpu.VMEM))
    dma = pltpu.SemaphoreType.DMA
    units = (ROWS // QUAD, QUAD, LANES)
    block = (ROWS, LANES)
    piece = (ROWS // 4, LANES)
    hops = 4 * (2 * (NY // 2) - 1)
    scratch = [
        pltpu.VMEM((HH, L), F32), pltpu.VMEM((1, HH), F32),
        pltpu.VMEM((4, VR), F32), pltpu.VMEM((4, conv_b.shape[0]), F32), pltpu.VMEM((4, conv_b.shape[0]), F32),
        pltpu.VMEM((1, VR), F32), pltpu.VMEM((TP, features // TP), F32),
        pltpu.VMEM((2, tokens), jnp.int32), pltpu.VMEM((2, tokens), F32),
        pltpu.VMEM((VR, L), BF16), pltpu.VMEM((VR, L), BF16),
        pltpu.VMEM((NSTATE, L), BF16), pltpu.VMEM((NSTATE, L), BF16),
        pltpu.VMEM((tokens, features), BF16),
        pltpu.VMEM((FD, features), BF16), pltpu.VMEM((FD, features), BF16), pltpu.VMEM((FD, features), BF16),
        pltpu.VMEM((VR + 2 * NSTATE, LANES), BF16),
        pltpu.VMEM((2, tokens, ROWS), BF16),
        pltpu.VMEM(units, BF16), pltpu.VMEM(units, BF16), pltpu.VMEM((TP,) + block, BF16),
        pltpu.VMEM((ROWS, FD), F32), pltpu.VMEM((ROWS, FD), F32), pltpu.VMEM((ROWS, FD), BF16),
        pltpu.VMEM((NY, 2) + block, BF16), pltpu.VMEM((NY,) + block, BF16),
        pltpu.VMEM((hops,) + piece, BF16), pltpu.VMEM((hops,) + piece, BF16),
        pltpu.VMEM(units, BF16), pltpu.VMEM(units, BF16),
        pltpu.VMEM((VR, L), BF16), pltpu.VMEM((NSTATE, L), BF16), pltpu.VMEM((NSTATE, L), BF16),
        pltpu.VMEM((L, L), F32), pltpu.VMEM((8, L), F32), pltpu.VMEM((L, 8), F32), pltpu.VMEM((VR, L), F32),
        pltpu.VMEM((EP, UR, LANES), BF16), pltpu.VMEM((EP, UR, LANES), BF16),
        pltpu.VMEM((EP, U, LANES), F32), pltpu.VMEM((EP, U, LANES), F32),
        dma((17,)), dma((3,)), dma((3,)), dma, dma, dma, dma, dma, dma,
        dma, dma((hops,)), dma, dma((NY, 2)), dma, dma((NY, 2)), dma, dma((hops,)), dma, dma,
    ]
    mixed, moe = pl.pallas_call(
        functools.partial(kernel_body, cfg),
        name="mixer_and_experts",
        out_shape=(
            pltpu.VMEM((VR, L), BF16),
            pltpu.VMEM((tokens, features // TP), BF16),
        ),
        in_specs=[hbm] * 17,
        out_specs=(vmem, vmem),
        scratch_shapes=scratch,
        compiler_params=pltpu.CompilerParams(
            collective_id=0, has_side_effects=True, vmem_limit_bytes=60 * 1024 * 1024
        ),
    )(
        x_in, z_in, dt_raw, decay_rate.reshape(1, HH), b_in, c_in, flipped(conv_x), flipped(conv_b), flipped(conv_c),
        head_gain.reshape(1, VR), moe_rows, moe_gain.reshape(TP, features // TP),
        flipped(routes), flipped(route_logit), flipped(w_gate), flipped(w_up), w_down,
    )
    return mixed, flipped(moe)


def solution(mesh):
    EP, TP = mesh.shape["ep"], mesh.shape["tp"]
    in_specs = (
        P("tp", "ep"), P("tp", "ep"), P("tp", "ep"), P("tp"), P(None, "ep"), P(None, "ep"),
        P("tp", None), P(), P(), P("tp"), P("ep", None), P(), P("ep", None), P("ep", None),
        P("ep", None, "tp"), P("ep", None, "tp"), P("ep", "tp", None),
    )
    return jax.shard_map(
        functools.partial(on_device, EP, TP),
        mesh=mesh,
        in_specs=in_specs,
        out_specs=(P("tp", "ep"), P("tp", "ep")),
        check_vma=False,
    )
```

time: 70.5 us -> 65.3 us (0.926)
  the two profiles are of different devices: /device:TPU:8 before, /device:TPU:6 now
where the time goes in v3:
time: 65.3 us; the launch traced here: 64.1 us
  Pallas kernels  62.2 us (95%)
  local copies, waits for them, and re-layouts  1.3 us (2%)
    pallas_call x1, Pallas kernels, on_device(): pl.pallas_call(functools.partial(kernel_body, cfg), name='mixer_and_exper...  62.2 us

profile of v3, /device:TPU:6, one launch (start us, length us, event | category | flops | bytes accessed | tf_op | source)
XLA Modules:
  0.0 64.1 jit_solution(4077642529257354480)
XLA Ops:
  0.6 62.2 %mixer_and_experts.1 = (bf16[256,384]{1,0:T(8,128)(2,1)S(1)}, bf16[160,128]{1,0:T(8,128)(2,1)S(1)}) custom-call(bf16[256,384]{1,0:T(8,128)(2,1)} %x_hbm.1, bf16[256,384]{1,0:T(8,128)(2,1)} %z_hbm.1, f32[4,384]{1,0:T(4,128)} %dt_hbm.1, f32[1,4]{1,0:T(1,128)} %bitcast.21, bf16[256,384]{1,0:T(8,128)(2,1)} %b_hbm.1, bf16[256,384]{1,0:T(8,128)(2,1)} %c_hbm.1, ...), custom_call_target="tpu_custom_call" | custom-call | tf_op jit(solution)/shard_map/mixer_and_experts/pallas_call | solution.py:562
  62.8 0.7 %copy.21 = bf16[256,384]{1,0:T(8,128)(2,1)} copy(bf16[256,384]{1,0:T(8,128)(2,1)S(1)} %get-tuple-element.6) | data formatting | bytes 393216
  63.5 0.6 copy.22

commit v4 on v3

--- a/solution.py
+++ b/solution.py
@@ -29,7 +29,7 @@
     rows_hbm, mgain_hbm, routes_hbm, logit_hbm, wg_hbm, wu_hbm, wd_hbm,
     mixed_ref, moe_ref,
     dt_ref, rate_ref, tapx_ref, tapb_ref, tapc_ref, hgain_ref, mgain_ref, routes_ref, logit_ref,
-    x_v, z_v, b_v, c_v, rows_v, wg_v, wu_v, wd_v, halo, pick, outbox, inbox, xall,
+    x_v, z_v, b_v, c_v, rows_v, wg_v, wu_v, wd_v, halo, rim_out, rim_in, pick, outbox, inbox, xall,
     gate_acc, up_acc, hid, part, sib, tosend, arrived, rout, rin,
     xs_v, bc_v, cc_v, gram_v, cum_v, colv, yloc, sout, sin, hout, hin,
     load_sem, halo_send, halo_recv, disp_send, disp_recv, st_send, st_recv, hb_send, hb_recv,
@@ -59,7 +59,9 @@
         dz, dx = offset
         return min(dz, NZ - dz) + min(dx, NX - dx)
 
-    offsets = sorted(((dz, dx) for dz in range(NZ) for dx in range(NX) if dz or dx), key=lambda o: -hops(o))
+    ranked = sorted(((dz, dx) for dz in range(NZ) for dx in range(NX)), key=hops)
+    seat = {offset: i for i, offset in enumerate(ranked)}
+    offsets = ranked[:0:-1]
     partners = [lax.rem(z_at + dz, NZ) * NX + lax.rem(x_at + dx, NX) for dz, dx in offsets]
 
     def at_ep(index):
@@ -138,12 +140,104 @@
 
     pl.semaphore_wait(barrier, EP - 1 + 3)
 
-    for tgt in partners:
-        rcopy(
-            outbox.at[pl.ds(tgt * UC, UC)], inbox.at[pl.ds(ep * UC, UC)], disp_send, disp_recv, at_ep(tgt)
-        ).start()
-
-    inbox[pl.ds(ep * UC, UC)] = outbox[pl.ds(ep * UC, UC)]
+    reaches = list(zip(offsets, partners))
+    for h in range(2):
+        for (dz, dx), tgt in reaches:
+            there = seat[(-dz) % NZ, (-dx) % NX]
+            if there // (EP // 2) == h:
+                rcopy(
+                    outbox.at[pl.ds(tgt * UC, UC)],
+                    inbox.at[pl.ds(there * UC, UC)],
+                    disp_send,
+                    disp_recv.at[h],
+                    at_ep(tgt),
+                ).start()
+
+    ready("x", "b", "c")
+    last = pl.ds(L - LANES, LANES)
+    rim_pick = (
+        lax.broadcasted_iota(jnp.int32, (16, LANES), 0) + (LANES - 16)
+        == lax.broadcasted_iota(jnp.int32, (16, LANES), 1)
+    ).astype(F32).astype(BF16)
+    edge = jnp.concatenate([x_v[:, last], b_v[:, last], c_v[:, last]], axis=0)
+    rim_out[...] = mm(rim_pick, edge, (((1,), (1,)), ((), ()))).astype(BF16)
+    halo_copy = rcopy(rim_out, rim_in, halo_send, halo_recv, at_ep(lax.rem(ep + 1, EP)))
+    halo_copy.start()
+    inbox[pl.ds(0, UC)] = outbox[pl.ds(ep * UC, UC)]
+
+    reach = NY // 2
+    streams = []
+    for q in range(4):
+        streams.append((q, 1, reach - q % 2))
+        streams.append((q, -1, reach - 1 + q % 2))
+
+    def lane(o, c):
+        return lax.rem(y + o + NY, NY) * 2 + c
+
+    def part_of(q):
+        return pl.ds(q * quarter, quarter)
+
+    def half_of(h):
+        return pl.ds(h * half_rows, half_rows)
+
+    phases = ((0, 3), (1, 2), (4, 7), (5, 6))
+    slots, count = {}, 0
+    for k in range(8):
+        for i in range(streams[k][2]):
+            slots[k, i] = count
+            count += 1
+
+    def live(p, i):
+        return [k for k in phases[p] if i < streams[k][2]]
+
+    def ring(k, i):
+        q, s, _ = streams[k]
+        blk = xall.at[lane(-s * i, core), part_of(q)]
+        return rcopy(blk, blk, ag_send, ag_recv.at[slots[k, i]], to_y(s))
+
+    def ring_recv(k, i):
+        q, s, _ = streams[k]
+        blk = xall.at[lane(-s * (i + 1), core), part_of(q)]
+        return rcopy(blk, blk, ag_send, ag_recv.at[slots[k, i]], to_y(s))
+
+    def cross(o, q):
+        blk = xall.at[lane(o, core), part_of(q)]
+        return rcopy(blk, blk, d2_send, d2_recv.at[o % NY, q // 2], sibling)
+
+    def cross_half(o, h, c):
+        blk = xall.at[lane(o, c), half_of(h)]
+        return rcopy(blk, blk, d2_send, d2_recv.at[o % NY, h], sibling)
+
+    def drain(i, p):
+        for k in live(p, i):
+            q, s, n = streams[k]
+            ring_recv(k, i).wait_recv()
+            if i + 1 < n:
+                ring(k, i + 1).start()
+            cross(-s * (i + 1), q).start()
+
+    def expand(*blocks, first=False):
+        for o, h in blocks:
+            cross_half(o, h, other).wait_recv()
+        for o, h in blocks:
+            yy = lax.rem(y + o + NY, NY)
+            rows = jnp.concatenate([xall[2 * yy, half_of(h), :], xall[2 * yy + 1, half_of(h), :]], axis=1)
+            ks = pl.ds(pl.multiple_of(yy * 2 * LANES, 2 * LANES), 2 * LANES)
+            for acc, w in ((gate_acc, wg_v), (up_acc, wu_v)):
+                prod = mm(rows, w[:, ks], (((1,), (1,)), ((), ())))
+                if first:
+                    acc[half_of(h), :] = prod
+                else:
+                    acc[half_of(h), :] += prod
+
+    def own_ready(h):
+        count = EP // 2 - 1 + h
+        wait_bytes(outbox.at[pl.ds(0, count * UC)], disp_recv.at[h])
+        xall[tp, half_of(h), :] = flat(inbox[pl.ds(h * (EP // 2) * UC, EP // 2 * UC)])
+        for p in (2 * h, 2 * h + 1):
+            for k in live(p, 0):
+                ring(k, 0).start()
+        cross_half(0, h, core).start()
 
     ready("logit", "dt", "rate")
     logit = logit_ref[...]
@@ -179,89 +273,6 @@
     tall = jnp.concatenate([cum, jnp.zeros((8 - HH, L), F32)], axis=0)
     colv[...] = jnp.transpose(tall)
 
-    reach = NY // 2
-    streams = []
-    for q in range(4):
-        streams.append((q, 1, reach - q % 2))
-        streams.append((q, -1, reach - 1 + q % 2))
-
-    def lane(o, c):
-        return lax.rem(y + o + NY, NY) * 2 + c
-
-    def part_of(q):
-        return pl.ds(q * quarter, quarter)
-
-    def half_of(h):
-        return pl.ds(h * half_rows, half_rows)
-
-    phases = ((0, 3), (4, 7), (1, 2), (5, 6))
-    slots, count = {}, 0
-    for k in range(8):
-        for i in range(streams[k][2]):
-            slots[k, i] = count
-            count += 1
-
-    def live(p, i):
-        return [k for k in phases[p] if i < streams[k][2]]
-
-    def ring(k, i):
-        q, s, _ = streams[k]
-        blk = xall.at[lane(-s * i, core), part_of(q)]
-        return rcopy(blk, blk, ag_send, ag_recv.at[slots[k, i]], to_y(s))
-
-    def ring_recv(k, i):
-        q, s, _ = streams[k]
-        blk = xall.at[lane(-s * (i + 1), core), part_of(q)]
-        return rcopy(blk, blk, ag_send, ag_recv.at[slots[k, i]], to_y(s))
-
-    def cross(o, q):
-        blk = xall.at[lane(o, core), part_of(q)]
-        return rcopy(blk, blk, d2_send, d2_recv.at[o % NY, q // 2], sibling)
-
-    def cross_half(o, h, c):
-        blk = xall.at[lane(o, c), half_of(h)]
-        return rcopy(blk, blk, d2_send, d2_recv.at[o % NY, h], sibling)
-
-    def drain(i, p):
-        for k in live(p, i):
-            q, s, n = streams[k]
-            ring_recv(k, i).wait_recv()
-            if i + 1 < n:
-                ring(k, i + 1).start()
-            cross(-s * (i + 1), q).start()
-
-    def expand(o, h, first=False):
-        cross_half(o, h, other).wait_recv()
-        yy = lax.rem(y + o + NY, NY)
-        rows = jnp.concatenate([xall[2 * yy, half_of(h), :], xall[2 * yy + 1, half_of(h), :]], axis=1)
-        ks = pl.ds(pl.multiple_of(yy * 2 * LANES, 2 * LANES), 2 * LANES)
-        for acc, w in ((gate_acc, wg_v), (up_acc, wu_v)):
-            prod = mm(rows, w[:, ks], (((1,), (1,)), ((), ())))
-            if first:
-                acc[half_of(h), :] = prod
-            else:
-                acc[half_of(h), :] += prod
-
-    wait_bytes(outbox.at[pl.ds(0, (EP - 1) * UC)], disp_recv)
-    xall[tp] = flat(inbox[...])
-    for p in range(4):
-        for k in live(p, 0):
-            ring(k, 0).start()
-    for h in range(2):
-        cross_half(0, h, core).start()
-    ready("x", "b", "c")
-    last = pl.ds(L - LANES, LANES)
-    halos = [
-        rcopy(x_v.at[:, last], halo.at[pl.ds(0, VR)], halo_send.at[0], halo_recv.at[0], at_ep(lax.rem(ep + 1, EP))),
-        rcopy(b_v.at[:, last], halo.at[pl.ds(VR, NSTATE)], halo_send.at[1], halo_recv.at[1], at_ep(lax.rem(ep + 1, EP))),
-        rcopy(
-            c_v.at[:, last], halo.at[pl.ds(VR + NSTATE, NSTATE)], halo_send.at[2], halo_recv.at[2], at_ep(lax.rem(ep + 1, EP))
-        ),
-    ]
-    for h in halos:
-        h.start()
-    ready("wg", "wu")
-
     started = (ep > 0).astype(F32)
 
     def conv(cur, rim, taps):
@@ -274,8 +285,8 @@
     kept = {}
 
     def taps_part():
-        for h in halos:
-            h.wait_recv()
+        halo_copy.wait_recv()
+        halo[...] = mm(rim_in[...], rim_pick, (((0,), (0,)), ((), ()))).astype(BF16)
         ready("tapx", "tapb", "tapc", "hgain")
         kept["bc"] = jnp.transpose(jnp.concatenate([tapb_ref[:, gsel], tapc_ref[:, gsel]], axis=0))
         kept["x"] = jnp.transpose(
@@ -291,6 +302,11 @@
             xs = xc * step[h : h + 1, :]
             xs_v[rows_h, :] = xs.astype(BF16)
             yloc[rows_h, :] = xs * tail[h : h + 1, :]
+
+    own_ready(0)
+    ready("wg", "wu")
+    expand((0, 0), first=True)
+    own_ready(1)
 
     def send_part():
         state = mm(yloc[...].astype(BF16), bc_v[...], (((1,), (1,)), ((), ())))
@@ -382,27 +398,26 @@
         lambda: local_part(range(2, HH)),
     ]
 
-    for h in range(2):
-        expand(0, h, first=True)
     far = reach - 1
     for i in range(far):
         for p in range(4):
             drain(i, p)
-            if i:
-                expand((i, -i, i, -i)[p], p // 2)
+            if (i, p) == (0, 1):
+                expand((0, 1), first=True)
+            if p == 3:
+                expand((i + 1, 0))
+            elif i:
+                expand(((-i, i, -i)[p], (0, 1, 1)[p]))
             if (i or p > 1) and pieces:
                 pieces.pop(0)()
-    if far:
-        expand(far, 0)
     for piece in pieces:
         piece()
     drain(far, 0)
     if far:
-        expand(-far, 0)
+        expand((-far, 0), (far, 1))
     drain(far, 1)
-    if far:
-        expand(far, 1)
-        expand(-far, 1)
+    drain(far, 2)
+    drain(far, 3)
 
     ready("wd")
 
@@ -415,13 +430,17 @@
             part.at[o % NY, other, half_of(h)], sib.at[o % NY, half_of(h)], ps_send, ps_recv.at[o % NY, h], sibling
         )
 
-    def project(o, h):
-        yy = lax.rem(y + o + NY, NY)
-        cols = pl.ds(pl.multiple_of(yy * 2 * LANES, 2 * LANES), 2 * LANES)
-        prod = mm(hid[half_of(h), :], wd_v[:, cols]).astype(BF16)
-        part[o % NY, 0, half_of(h), :] = prod[:, :LANES]
-        part[o % NY, 1, half_of(h), :] = prod[:, LANES:]
-        swap(o, h).start()
+    def project(*blocks):
+        prods = []
+        for o, h in blocks:
+            yy = lax.rem(y + o + NY, NY)
+            cols = pl.ds(pl.multiple_of(yy * 2 * LANES, 2 * LANES), 2 * LANES)
+            prods.append(mm(hid[half_of(h), :], wd_v[:, cols]).astype(BF16))
+        for (o, h), prod in zip(blocks, prods):
+            part[o % NY, 0, half_of(h), :] = prod[:, :LANES]
+            part[o % NY, 1, half_of(h), :] = prod[:, LANES:]
+        for o, h in blocks:
+            swap(o, h).start()
 
     swapped = set()
 
@@ -453,56 +472,50 @@
         for k in live(p, i):
             feed(k, i)
 
-    def project_for(i, side, h):
+    def sides(i, h):
         m = reach - 1 - i
-        if m > 0:
-            project(side * m, h)
-        elif m == 0 and side < 0:
-            project(0, h)
-
+        return [] if m < 0 else [(o, h) for o in sorted({-m, m})]
+
+    expand((reach, 0))
+    activate(0)
+    project((reach, 0))
+    expand(*([(-far, 1)] if far else []), (reach, 1))
+    activate(1)
+    first, second = sides(0, 0), sides(0, 1)
+    project((reach, 1), *first[:1])
+    feed_all(0, 0)
+    project(*first[1:], *second[:1])
+    feed_all(2, 0)
+    project(*second[1:])
+    feed_all(1, 0)
+    project(*sides(1, 0))
+    feed_all(3, 0)
+    for i in range(1, reach):
+        for at, p in enumerate((0, 2, 1, 3)):
+            feed_all(p, i)
+            coming = ([], sides(i, 1), [], sides(i + 1, 0))[at]
+            if coming:
+                project(*coming)
+            if (i, at) == (1, 2 if far > 1 else 0):
+                prefix_part()
+    units = quarter // QUAD
     for h in range(2):
-        expand(reach, h)
-        activate(h)
-        project(reach, h)
-    feed_all(0, 0)
-    project_for(0, -1, 0)
-    feed_all(1, 0)
-    project_for(0, 1, 0)
-    project_for(0, -1, 1)
-    project_for(0, 1, 1)
-    feed_all(2, 0)
-    project_for(1, -1, 0)
-    feed_all(3, 0)
-    project_for(1, 1, 0)
-    for i in range(1, reach):
-        for p in range(4):
-            feed_all(p, i)
-            if p < 2:
-                project_for(i, (-1, 1)[p], 1)
-            else:
-                project_for(i + 1, (-1, 1)[p - 2], 0)
-            if (i, p) == (min(2, far), 1):
-                prefix_part()
-    if reach == 1:
-        project(0, 1)
-    units = quarter // QUAD
-    for q in range(4):
-        value = pair_sum(0, q)
-        for k in (2 * q, 2 * q + 1):
-            if streams[k][2] > 0:
-                value = value + came(k, streams[k][2] - 1)
-        put(rout.at[pl.ds(q * units, units)], value.astype(BF16))
-
-    for tgt in partners:
-        rcopy(
-            rout.at[pl.ds(tgt * UC, UC)], rin.at[pl.ds(ep * UC, UC)], rt_send, rt_recv, at_ep(tgt)
-        ).start()
-
-    rin[pl.ds(ep * UC, UC)] = rout[pl.ds(ep * UC, UC)]
+        for q in (2 * h, 2 * h + 1):
+            value = pair_sum(0, q)
+            for k in (2 * q, 2 * q + 1):
+                if streams[k][2] > 0:
+                    value = value + came(k, streams[k][2] - 1)
+            put(rout.at[pl.ds(q * units, units)], value.astype(BF16))
+        for offset, tgt in reaches:
+            if seat[offset] // (EP // 2) == h:
+                rcopy(
+                    rout.at[pl.ds(seat[offset] * UC, UC)], rin.at[pl.ds(ep * UC, UC)], rt_send, rt_recv, at_ep(tgt)
+                ).start()
+    rin[pl.ds(ep * UC, UC)] = rout[pl.ds(0, UC)]
+
     final_part()
     wait_bytes(outbox.at[pl.ds(0, (EP - 1) * UC)], disp_send)
-    for h in halos:
-        h.wait_send()
+    halo_copy.wait_send()
     wait_bytes(sout.at[pl.ds(0, EP - 1)], st_send)
     wait_bytes(hout.at[pl.ds(0, EP - 1)], hb_send)
     wait_bytes(xall.at[pl.ds(0, NY - 1)], ag_send)
@@ -514,6 +527,17 @@
     back = flat(rin[...])
     moe_ref[...] = (mm(pick[0], back) + mm(pick[1], back)).astype(BF16)
     wait_bytes(rout.at[pl.ds(0, (EP - 1) * UC)], rt_send)
+
+
+def place_body(mixed_ref, moe_ref, mixed_out, moe_out, sem):
+    copies = [
+        pltpu.make_async_copy(mixed_ref, mixed_out, sem.at[0]),
+        pltpu.make_async_copy(moe_ref, moe_out, sem.at[1]),
+    ]
+    for copy in copies:
+        copy.start()
+    for copy in copies:
+        copy.wait()
 
 
 def on_device(EP, TP, *args):
@@ -546,6 +570,7 @@
         pltpu.VMEM((tokens, features), BF16),
         pltpu.VMEM((FD, features), BF16), pltpu.VMEM((FD, features), BF16), pltpu.VMEM((FD, features), BF16),
         pltpu.VMEM((VR + 2 * NSTATE, LANES), BF16),
+        pltpu.VMEM((16, VR + 2 * NSTATE), BF16), pltpu.VMEM((16, VR + 2 * NSTATE), BF16),
         pltpu.VMEM((2, tokens, ROWS), BF16),
         pltpu.VMEM(units, BF16), pltpu.VMEM(units, BF16), pltpu.VMEM((TP,) + block, BF16),
         pltpu.VMEM((ROWS, FD), F32), pltpu.VMEM((ROWS, FD), F32), pltpu.VMEM((ROWS, FD), BF16),
@@ -556,7 +581,7 @@
         pltpu.VMEM((L, L), F32), pltpu.VMEM((8, L), F32), pltpu.VMEM((L, 8), F32), pltpu.VMEM((VR, L), F32),
         pltpu.VMEM((EP, UR, LANES), BF16), pltpu.VMEM((EP, UR, LANES), BF16),
         pltpu.VMEM((EP, U, LANES), F32), pltpu.VMEM((EP, U, LANES), F32),
-        dma((17,)), dma((3,)), dma((3,)), dma, dma, dma, dma, dma, dma,
+        dma((17,)), dma, dma, dma, dma((2,)), dma, dma, dma, dma,
         dma, dma((hops,)), dma, dma((NY, 2)), dma, dma((NY, 2)), dma, dma((hops,)), dma, dma,
     ]
     mixed, moe = pl.pallas_call(
@@ -577,6 +602,14 @@
         head_gain.reshape(1, VR), moe_rows, moe_gain.reshape(TP, features // TP),
         flipped(routes), flipped(route_logit), flipped(w_gate), flipped(w_up), w_down,
     )
+    mixed, moe = pl.pallas_call(
+        place_body,
+        name="place",
+        out_shape=(jax.ShapeDtypeStruct(mixed.shape, BF16), jax.ShapeDtypeStruct(moe.shape, BF16)),
+        in_specs=[vmem, vmem],
+        out_specs=(hbm, hbm),
+        scratch_shapes=[dma((2,))],
+    )(*(pltpu.with_memory_space_constraint(o, pltpu.VMEM) for o in (mixed, moe)))
     return mixed, flipped(moe)
 
 

time: 65.3 us -> 63.2 us (0.968)
  local copies, waits for them, and re-layouts: 1.3 us -> 0 us
  Pallas kernels: 62.2 us -> 61.4 us
    pallas_call x1, Pallas kernels: 62.2 us -> 60.7 us  [on_device(): pl.pallas_call(functools.partial(kernel_body, cfg), name='mixer_and_exper...]
    unnamed x2 -> x0, local copies, waits for them, and re-layouts: 1.3 us -> none
    pallas_call x0 -> x1, Pallas kernels: none -> 0.7 us  [on_device(): pl.pallas_call(place_body, name='place', out_shape=(jax.ShapeDtypeStruct(...]
where the time goes in v4:
time: 63.2 us; the launch traced here: 62.1 us
  Pallas kernels  61.4 us (97%)
  between operations  0.65 us (1%)
    pallas_call x1, Pallas kernels, on_device(): pl.pallas_call(functools.partial(kernel_body, cfg), name='mixer_and_exper...  60.7 us

profile of v4, /device:TPU:6, one launch (start us, length us, event | category | flops | bytes accessed | tf_op | source)
XLA Modules:
  0.0 62.1 jit_solution(16446185496732449981)
XLA Ops:
  0.6 60.7 %mixer_and_experts.1 = (bf16[256,384]{1,0:T(8,128)(2,1)S(1)}, bf16[160,128]{1,0:T(8,128)(2,1)S(1)}) custom-call(bf16[256,384]{1,0:T(8,128)(2,1)} %x_hbm.1, bf16[256,384]{1,0:T(8,128)(2,1)} %z_hbm.1, f32[4,384]{1,0:T(4,128)} %dt_hbm.1, f32[1,4]{1,0:T(1,128)} %bitcast.20, bf16[256,384]{1,0:T(8,128)(2,1)} %b_hbm.1, bf16[256,384]{1,0:T(8,128)(2,1)} %c_hbm.1, ...), custom_call_target="tpu_custom_call" | custom-call | tf_op jit(solution)/shard_map/mixer_and_experts/pallas_call | solution.py:587
  61.4 0.7 %place.1 = (bf16[256,384]{1,0:T(8,128)(2,1)}, bf16[160,128]{1,0:T(8,128)(2,1)}) custom-call(bf16[256,384]{1,0:T(8,128)(2,1)S(1)} %get-tuple-element.6.mixed_ref, bf16[160,128]{1,0:T(8,128)(2,1)S(1)} %get-tuple-element.7.moe_ref), custom_call_target="tpu_custom_call" | custom-call | tf_op jit(solution)/shard_map/place/pallas_call | solution.py:605

commit v5 on v4

--- a/solution.py
+++ b/solution.py
@@ -190,15 +190,20 @@
     def live(p, i):
         return [k for k in phases[p] if i < streams[k][2]]
 
+    pair_at = {}
+    for p in range(4):
+        for i in range(reach):
+            if live(p, i):
+                pair_at[p, i] = len(pair_at)
+    phase_of = {k: p for p in range(4) for k in phases[p]}
+
+    def pair_index(k, i):
+        return pair_at[phase_of[k], i]
+
     def ring(k, i):
         q, s, _ = streams[k]
         blk = xall.at[lane(-s * i, core), part_of(q)]
-        return rcopy(blk, blk, ag_send, ag_recv.at[slots[k, i]], to_y(s))
-
-    def ring_recv(k, i):
-        q, s, _ = streams[k]
-        blk = xall.at[lane(-s * (i + 1), core), part_of(q)]
-        return rcopy(blk, blk, ag_send, ag_recv.at[slots[k, i]], to_y(s))
+        return rcopy(blk, blk, ag_send, ag_recv.at[pair_index(k, i)], to_y(s))
 
     def cross(o, q):
         blk = xall.at[lane(o, core), part_of(q)]
@@ -209,11 +214,13 @@
         return rcopy(blk, blk, d2_send, d2_recv.at[o % NY, h], sibling)
 
     def drain(i, p):
+        if live(p, i):
+            wait_bytes(xall.at[0, half_of(0)], ag_recv.at[pair_at[p, i]])
         for k in live(p, i):
-            q, s, n = streams[k]
-            ring_recv(k, i).wait_recv()
-            if i + 1 < n:
+            if i + 1 < streams[k][2]:
                 ring(k, i + 1).start()
+        for k in live(p, i):
+            q, s, _ = streams[k]
             cross(-s * (i + 1), q).start()
 
     def expand(*blocks, first=False):
@@ -326,9 +333,7 @@
                 extra.append(jnp.zeros((UR - U - 8, LANES), F32))
             sout[u] = jnp.concatenate(extra, axis=0).astype(BF16)
 
-        @pl.loop(1, EP)
-        def _(d):
-            tgt = lax.rem(ep + d, EP)
+        for tgt in partners:
             rcopy(sout.at[tgt], sin.at[ep], st_send, st_recv, at_ep(tgt)).start()
 
         sin[ep] = sout[ep]
@@ -367,9 +372,7 @@
             keep = jnp.exp(blk[U : U + 1] + blk[U + 1 : U + 2] + blk[U + 2 : U + 3])
             held = keep * held + blk[:U]
 
-        @pl.loop(1, EP)
-        def _(d):
-            tgt = lax.rem(ep + d, EP)
+        for tgt in partners:
             rcopy(hout.at[tgt], hin.at[ep], hb_send, hb_recv, at_ep(tgt)).start()
 
         hin[ep] = hout[ep]
@@ -392,11 +395,8 @@
         lambda: value_part(range(HH // 2)),
         lambda: value_part(range(HH // 2, HH)),
         send_part,
-        gram_part,
-        lambda: local_part([0]),
-        lambda: local_part([1]),
-        lambda: local_part(range(2, HH)),
     ]
+    later = [gram_part] + [functools.partial(local_part, [h]) for h in range(HH)]
 
     far = reach - 1
     for i in range(far):
@@ -454,10 +454,15 @@
 
     def push(k, i):
         j = slots[k, i]
-        return rcopy(tosend.at[j], arrived.at[j], rs_send, rs_recv.at[j], to_y(streams[k][1]))
+        return rcopy(tosend.at[j], arrived.at[j], rs_send, rs_recv.at[pair_index(k, i)], to_y(streams[k][1]))
+
+    landed = set()
 
     def came(k, i):
-        push(k, i).wait_recv()
+        at = pair_index(k, i)
+        if at not in landed:
+            wait_bytes(arrived.at[pl.ds(0, 2)], rs_recv.at[at])
+            landed.add(at)
         return arrived[slots[k, i]].astype(F32)
 
     def feed(k, i):
@@ -479,27 +484,32 @@
     expand((reach, 0))
     activate(0)
     project((reach, 0))
-    expand(*([(-far, 1)] if far else []), (reach, 1))
+    if far:
+        expand((-far, 1))
+    expand((reach, 1))
     activate(1)
-    first, second = sides(0, 0), sides(0, 1)
-    project((reach, 1), *first[:1])
+    project((reach, 1))
+    project(*sides(0, 1))
+    feed_all(2, 0)
     feed_all(0, 0)
-    project(*first[1:], *second[:1])
-    feed_all(2, 0)
-    project(*second[1:])
+    project(*sides(0, 0))
+    feed_all(3, 0)
+    project(*sides(1, 1))
     feed_all(1, 0)
-    project(*sides(1, 0))
-    feed_all(3, 0)
     for i in range(1, reach):
-        for at, p in enumerate((0, 2, 1, 3)):
+        for at, p in enumerate((2, 0, 3, 1)):
             feed_all(p, i)
-            coming = ([], sides(i, 1), [], sides(i + 1, 0))[at]
+            coming = ([], sides(i, 0), [], sides(i + 1, 1))[at]
             if coming:
                 project(*coming)
             if (i, at) == (1, 2 if far > 1 else 0):
                 prefix_part()
+            elif later:
+                later.pop(0)()
+    for piece in later:
+        piece()
     units = quarter // QUAD
-    for h in range(2):
+    for h in (1, 0):
         for q in (2 * h, 2 * h + 1):
             value = pair_sum(0, q)
             for k in (2 * q, 2 * q + 1):
@@ -582,7 +592,7 @@
         pltpu.VMEM((EP, UR, LANES), BF16), pltpu.VMEM((EP, UR, LANES), BF16),
         pltpu.VMEM((EP, U, LANES), F32), pltpu.VMEM((EP, U, LANES), F32),
         dma((17,)), dma, dma, dma, dma((2,)), dma, dma, dma, dma,
-        dma, dma((hops,)), dma, dma((NY, 2)), dma, dma((NY, 2)), dma, dma((hops,)), dma, dma,
+        dma, dma((hops // 2,)), dma, dma((NY, 2)), dma, dma((NY, 2)), dma, dma((hops // 2,)), dma, dma,
     ]
     mixed, moe = pl.pallas_call(
         functools.partial(kernel_body, cfg),

time: 63.2 us -> 63.1 us (level)
  no operation moved by 1% of the time
where the time goes in v5:
time: 63.1 us; the launch traced here: 62.3 us
  Pallas kernels  61.7 us (98%)
  between operations  0.65 us (1%)
    pallas_call x1, Pallas kernels, on_device(): pl.pallas_call(functools.partial(kernel_body, cfg), name='mixer_and_exper...  61 us

profile of v5, /device:TPU:6, one launch (start us, length us, event | category | flops | bytes accessed | tf_op | source)
XLA Modules:
  0.0 62.3 jit_solution(1315045518349531802)
XLA Ops:
  0.6 61.0 %mixer_and_experts.1 = (bf16[256,384]{1,0:T(8,128)(2,1)S(1)}, bf16[160,128]{1,0:T(8,128)(2,1)S(1)}) custom-call(bf16[256,384]{1,0:T(8,128)(2,1)} %x_hbm.1, bf16[256,384]{1,0:T(8,128)(2,1)} %z_hbm.1, f32[4,384]{1,0:T(4,128)} %dt_hbm.1, f32[1,4]{1,0:T(1,128)} %bitcast.20, bf16[256,384]{1,0:T(8,128)(2,1)} %b_hbm.1, bf16[256,384]{1,0:T(8,128)(2,1)} %c_hbm.1, ...), custom_call_target="tpu_custom_call" | custom-call | tf_op jit(solution)/shard_map/mixer_and_experts/pallas_call | solution.py:597
  61.6 0.7 %place.1 = (bf16[256,384]{1,0:T(8,128)(2,1)}, bf16[160,128]{1,0:T(8,128)(2,1)}) custom-call(bf16[256,384]{1,0:T(8,128)(2,1)S(1)} %get-tuple-element.6.mixed_ref, bf16[160,128]{1,0:T(8,128)(2,1)S(1)} %get-tuple-element.7.moe_ref), custom_call_target="tpu_custom_call" | custom-call | tf_op jit(solution)/shard_map/place/pallas_call | solution.py:615
